TPU v7x, 512 devices: a whole 4x8x8 slice. The times are simulated.
512 devices in a mesh: ep: 32 (over z, x), tp: 16 (over y, core).
Axes of the slice: x: 4, y: 8, z: 8, core: 2. Of those that a mesh axis runs over, the one named last changes fastest.
Arguments:
- residual: bfloat16 [256, 2048], P(None, 'ep'), may hold values from -40 to 40
- norm_gain: float32 [2048], P('ep'), may hold values from 0.1 to 1.9
- query_weight: bfloat16 [2048, 2048], P('ep', 'tp'), may hold values from -0.125 to 0.125
- key_weight: bfloat16 [2048, 2048], P('ep', 'tp'), may hold values from -0.125 to 0.125
- value_weight: bfloat16 [2048, 4096], P('ep', 'tp'), may hold values from -0.125 to 0.125
- gate_weight: bfloat16 [2048, 4096], P('ep', 'tp'), may hold values from -0.125 to 0.125
- out_weight: bfloat16 [4096, 2048], P('tp', 'ep'), may hold values from -0.09375 to 0.09375
- prior_state: float32 [256, 16, 128, 256], P('ep', 'tp'), may hold values from -3 to 3
- lengths: int32 [256], P('ep'), may hold values from 1024 to 16383
- ffn_gain: float32 [2048], replicated, may hold values from 0.1 to 1.9
- expert_gate: bfloat16 [32, 2048, 2048], P('ep', None, 'tp'), may hold values from -0.5 to 0.5
- expert_up: bfloat16 [32, 2048, 2048], P('ep', None, 'tp'), may hold values from -0.5 to 0.5
- expert_down: bfloat16 [32, 2048, 2048], P('ep', 'tp'), may hold values from -0.03125 to 0.03125
- route_ids: int32 [256, 4], replicated, may hold values from 0 to 31, all different within a row; in each aligned block of 8 rows (0 to 7, 8 to 15, ...) at most 2 rows name the same one
- route_weight: float32 [256, 4], replicated, may hold values from 0.1 to 1
- dense_gate: bfloat16 [2048, 2048], P('ep', 'tp'), may hold values from -0.125 to 0.125
- dense_up: bfloat16 [2048, 2048], P('ep', 'tp'), may hold values from -0.125 to 0.125
- dense_down: bfloat16 [2048, 2048], P('tp', 'ep'), may hold values from -0.25 to 0.25
- mix_vector: bfloat16 [2048], P('ep'), may hold values from -0.125 to 0.125
Outputs:
- layer_out: bfloat16 [256, 2048], P(None, 'ep')
- new_state: float32 [256, 16, 128, 256], P('ep', 'tp')
Inputs may be any that keep to these rules, and one draw needn't show every extreme that they name: `route_ids`: each row names 4 different experts; within each aligned block of 8 rows no expert is named by more than 2 rows, and in some block one expert is named by exactly 2 rows.
All inputs are finite; a program needn't handle non-finite values.
Results may differ from a plain program's by a relative error of at most 0.02.
Values may be sent and summed in bfloat16 or wider, within the bound.
No kernel may reach another device: no remote copies, remote signals or barrier semaphores. Data moves between devices by JAX's collectives and lax.ppermute only.
A program may use at most 64 MiB of HBM per device.

v0:
```python
import math

import jax
import jax.numpy as jnp
from jax import lax
from jax.sharding import PartitionSpec as P

D = 2048
KEY_DIM = 128
VAL_DIM = 256


norm_eps = 1e-06
clamp_limit = 7.0
gate_alpha = 1.702


def split_up(value, dim, peers):
    shape = value.shape
    pieces = value.reshape(*shape[:dim], peers, shape[dim] // peers, *shape[dim + 1 :])
    return jnp.moveaxis(pieces, dim, 0)


def summed_on_arrival(value, axis, dim):
    pieces = split_up(value, dim, lax.axis_size(axis))
    arrived = lax.all_to_all(pieces, axis, split_axis=0, concat_axis=0, tiled=True)
    return arrived.sum(axis=0)


def in_one_piece(arrays, axis, dim, along):
    widths = [math.prod(a.shape[along:]) for a in arrays]
    both = jnp.concatenate(
        [a.reshape(*a.shape[:along], w) for a, w in zip(arrays, widths)], axis=along
    )
    filled = summed_on_arrival(both, axis, dim)
    pieces = jnp.split(filled, [sum(widths[:k]) for k in range(1, len(widths))], axis=along)
    return tuple(
        (b.reshape(*filled.shape[:along], *a.shape[along:]) for a, b in zip(arrays, pieces))
    )


def from_everyone(value, axis):
    peers = lax.axis_size(axis)
    return lax.all_to_all(
        jnp.broadcast_to(value[None], (peers, *value.shape)), axis, 0, 0, tiled=True
    )


def laid_out(pieces, dim):
    shape = list(pieces.shape[1:])
    shape[dim] *= pieces.shape[0]
    return jnp.moveaxis(pieces, 0, dim).reshape(shape)


def gather_directly(value, axis, dim):
    pieces = from_everyone(value, axis)
    return laid_out(pieces, dim)


def total_of_pieces(value, axis):
    pieces = lax.all_gather(value, axis).astype(jnp.float32)
    return pieces.sum(axis=0)


def sum_at_owner(value, axis, dim):
    pieces = split_up(value, dim, lax.axis_size(axis))
    arrived = lax.all_to_all(pieces, axis, split_axis=0, concat_axis=0, tiled=True)
    return arrived.astype(jnp.float32).sum(axis=0)


def padded_to(lines, peers):
    spare = -lines.shape[0] % peers
    if not spare:
        return lines
    return jnp.concatenate([lines, jnp.zeros((spare, *lines.shape[1:]), lines.dtype)])


def nested_sum(value, axes):
    lines = value.reshape(-1, value.shape[-1])
    own = sum_at_owner(padded_to(lines, lax.axis_size(axes)), axes, 0)
    whole = gather_directly(own.astype(jnp.bfloat16), axes, 0)
    return whole[: len(lines)].reshape(value.shape).astype(jnp.float32)


def sum_by_parts(value, axes):
    padded = padded_to(value, lax.axis_size(axes))
    whole = gather_directly(summed_on_arrival(padded, axes, 0), axes, 0)
    return lax.slice_in_dim(whole, 0, len(value)).reshape(value.shape)


def in_one(arrays, axis):
    ends = [0]
    for a in arrays:
        ends.append(ends[-1] + a.size)
    subtotal = sum_by_parts(jnp.concatenate([a.ravel() for a in arrays]), axis)
    return tuple((subtotal[b:e].reshape(a.shape) for a, b, e in zip(arrays, ends, ends[1:])))


def rotate_half(vectors, positions):
    half_dim = vectors.shape[-1] // 2
    inverse = 1.0 / 10000.0 ** jnp.linspace(0.0, 1.0, half_dim, dtype=jnp.float32)
    angles = positions.astype(jnp.float32)[:, None] * inverse[None, :]
    cosine = jnp.cos(angles)[:, None, :]
    sine_part = jnp.sin(angles)[:, None, :]
    first_half = vectors[..., :half_dim]
    second_half = vectors[..., half_dim:]
    return jnp.concatenate(
        [
            first_half * cosine - second_half * sine_part,
            second_half * cosine + first_half * sine_part,
        ],
        axis=-1,
    )


def slot_index(route_ids, groups, capacity, experts):
    pair_ids = route_ids.reshape(groups, -1)
    labels = jnp.arange(experts, dtype=jnp.int32)
    onehot = (pair_ids[:, :, None] == labels[None, None, :]).astype(jnp.int32)
    earlier = jnp.cumsum(onehot, axis=1) - onehot
    within = jnp.sum(earlier * onehot, axis=2)
    offset = jnp.arange(groups, dtype=jnp.int32)[:, None] * capacity
    return (pair_ids * (groups * capacity) + offset + within).reshape(-1)


def source_rows(target, total_rows, topk_count, table_size):
    owners = jnp.arange(target.shape[0], dtype=jnp.int32) // topk_count
    return jnp.full((table_size,), total_rows, jnp.int32).at[target].set(owners)


def rounded_product(left_rows, right_rows):
    partial_value = jnp.dot(left_rows, right_rows, preferred_element_type=jnp.float32)
    return lax.optimization_barrier(partial_value.astype(jnp.bfloat16))


def per_device(
    residual,
    norm_gain,
    query_weight,
    key_weight,
    value_weight,
    gate_weight,
    out_weight,
    prior_state,
    lengths,
    ffn_gain,
    expert_gate,
    expert_up,
    expert_down,
    route_ids,
    route_weight,
    dense_gate,
    dense_up,
    dense_down,
    mix_vector,
):
    ep_count = lax.axis_size("ep")
    ep_index = lax.axis_index("ep")
    batch_rows, local_width = residual.shape
    own_rows = batch_rows // ep_count
    topk_count = route_ids.shape[1]
    residual_float = residual.astype(jnp.float32)
    squares = jnp.sum(residual_float * residual_float, axis=1)
    normed_in = (residual_float * norm_gain).astype(jnp.bfloat16)
    all_weights = jnp.concatenate([query_weight, key_weight, value_weight, gate_weight], axis=1)
    whole_terms = jnp.dot(normed_in, all_weights, preferred_element_type=jnp.float32)
    projected, own_squares = in_one_piece((whole_terms, squares), "ep", 0, 1)
    row_scale = lax.rsqrt(own_squares / D + norm_eps)[:, None]
    key_cols = query_weight.shape[1]
    value_cols = value_weight.shape[1]
    heads_here = key_cols // KEY_DIM
    projected = projected * row_scale
    query_rot = rotate_half(projected[:, :key_cols].reshape(own_rows, heads_here, KEY_DIM), lengths)
    key_rot = rotate_half(
        projected[:, key_cols : 2 * key_cols].reshape(own_rows, heads_here, KEY_DIM), lengths
    ) * KEY_DIM ** (-0.5)
    values = projected[:, 2 * key_cols : 2 * key_cols + value_cols].reshape(
        own_rows, heads_here, VAL_DIM
    )
    gate_pre = projected[:, 2 * key_cols + value_cols :].reshape(own_rows, heads_here, VAL_DIM)
    head_ids = lax.axis_index("tp") * heads_here + jnp.arange(heads_here, dtype=jnp.int32)
    decay_rate = 1.0 - jnp.exp2(-1.0 - 0.5 * head_ids.astype(jnp.float32))
    new_state = (
        decay_rate[None, :, None, None] * prior_state
        + key_rot[:, :, :, None] * values[:, :, None, :]
    )
    state_read = jnp.einsum("bhk,bhkv->bhv", query_rot, new_state, precision=lax.Precision.HIGHEST)
    normed = state_read * lax.rsqrt(
        jnp.mean(state_read * state_read, axis=-1, keepdims=True) + norm_eps
    )
    gated_out = (
        (normed * jax.nn.silu(gate_pre))
        .astype(jnp.bfloat16)
        .reshape(own_rows, heads_here * VAL_DIM)
    )
    head_terms = rounded_product(gather_directly(gated_out, "ep", 0), out_weight)
    attn_out = total_of_pieces(head_terms.astype(jnp.float32).astype(jnp.bfloat16), "tp").astype(
        jnp.float32
    )
    after_mixer = (residual_float + attn_out).astype(jnp.bfloat16)
    capacity = max(2, 2 * own_rows * topk_count // ep_count)
    slot_count = ep_count * capacity
    target = slot_index(route_ids, ep_count, capacity, ep_count)
    slot_source = source_rows(target, batch_rows, topk_count, ep_count * slot_count)
    padded = jnp.concatenate([after_mixer, jnp.zeros((1, local_width), jnp.bfloat16)], axis=0)
    outgoing = padded[slot_source].reshape(ep_count, slot_count, local_width)
    arrived = lax.all_to_all(outgoing, "ep", split_axis=0, concat_axis=2, tiled=True)[0]
    rows_float = arrived.astype(jnp.float32)
    row_norm = lax.rsqrt(jnp.mean(rows_float * rows_float, axis=1, keepdims=True) + norm_eps)
    normed_rows = (rows_float * ffn_gain).astype(jnp.bfloat16)
    gate_val = jnp.minimum(
        jnp.dot(normed_rows, expert_gate[0], preferred_element_type=jnp.float32) * row_norm,
        clamp_limit,
    )
    up_val = jnp.clip(
        jnp.dot(normed_rows, expert_up[0], preferred_element_type=jnp.float32) * row_norm,
        -clamp_limit,
        clamp_limit,
    )
    hidden = ((up_val + 1.0) * gate_val * jax.nn.sigmoid(gate_alpha * gate_val)).astype(
        jnp.bfloat16
    )
    expert_part = rounded_product(hidden, expert_down[0]).astype(jnp.float32)
    expert_sum = nested_sum(expert_part.astype(jnp.bfloat16), "tp").astype(jnp.bfloat16)
    returned = lax.all_to_all(expert_sum[None], "ep", split_axis=2, concat_axis=0, tiled=True)
    picked = returned.reshape(ep_count * slot_count, local_width)[target]
    picked = picked.reshape(batch_rows, topk_count, local_width).astype(jnp.float32)
    routed = jnp.sum(picked * route_weight[:, :, None], axis=1)
    after_float = after_mixer.astype(jnp.float32)
    gain_here = lax.dynamic_slice_in_dim(ffn_gain, ep_index * local_width, local_width, 0)
    normed_ffn = (after_float * gain_here).astype(jnp.bfloat16)
    dense_cols = dense_gate.shape[1]
    both_terms = jnp.dot(
        normed_ffn,
        jnp.concatenate([dense_gate, dense_up], axis=1),
        preferred_element_type=jnp.float32,
    )
    mix_term = jnp.dot(normed_ffn, mix_vector, preferred_element_type=jnp.float32)
    both_terms, ffn_squares, mix_logit = in_one(
        (both_terms, jnp.sum(after_float * after_float, axis=1), mix_term), "ep"
    )
    ffn_scale = lax.rsqrt(ffn_squares / D + norm_eps)[:, None]
    dense_act = (
        jax.nn.silu(both_terms[:, :dense_cols] * ffn_scale)
        * (both_terms[:, dense_cols:] * ffn_scale)
    ).astype(jnp.bfloat16)
    dense_part = rounded_product(dense_act, dense_down).astype(jnp.float32)
    dense_out = total_of_pieces(dense_part.astype(jnp.bfloat16), "tp").astype(jnp.float32)
    dense_mix = jax.nn.sigmoid(ffn_scale[:, 0] * mix_logit)
    layer_out = (after_float + routed + dense_mix[:, None] * dense_out).astype(jnp.bfloat16)
    return (layer_out, new_state)


def solution(mesh):
    placed = (
        P(None, "ep"),
        P("ep"),
        P("ep", "tp"),
        P("ep", "tp"),
        P("ep", "tp"),
        P("ep", "tp"),
        P("tp", "ep"),
        P("ep", "tp", None, None),
        P("ep"),
        P(),
        P("ep", None, "tp"),
        P("ep", None, "tp"),
        P("ep", "tp", None),
        P(),
        P(),
        P("ep", "tp"),
        P("ep", "tp"),
        P("tp", "ep"),
        P("ep"),
    )
    return jax.shard_map(
        per_device,
        mesh=mesh,
        in_specs=placed,
        out_specs=(P(None, "ep"), P("ep", "tp", None, None)),
        check_vma=False,
    )
```

profile of v0, /device:TPU:1, one launch (start us, length us, event | category | flops | bytes accessed | tf_op | source)
XLA Modules:
  0.0 217.2 jit_solution(9277276090891454630)
XLA Ops:
  0.6 0.9 copy.80
  1.8 0.2 concatenate.51
  2.0 0.5 copy-done.5
  2.5 0.2 convolution_bitcast_fusion
  2.7 1.0 pad_maximum_fusion
  3.7 13.8 %all-to-all-start = ((f32[32,8,769]{2,1,0:T(8,128)}), f32[32,8,769]{2,1,0:T(8,128)S(1)}, u32[]{:S(2)}, u32[]{:S(2)}) async-start(f32[32,8,769]{2,1,0:T(8,128)} %pad_maximum_fusion), calls=%async_computation | async-start | bytes 1835008 | tf_op jit(solution)/shard_map/all_to_all | solution.py:26
  18.0 1.0 fusion.97
  19.7 21.4 %all-to-all-done = f32[32,8,769]{2,1,0:T(8,128)S(1)} async-done(((f32[32,8,769]{2,1,0:T(8,128)}), f32[32,8,769]{2,1,0:T(8,128)S(1)}, u32[]{:S(2)}, u32[]{:S(2)}) %all-to-all-start) | async-done | bytes 787488 | tf_op jit(solution)/shard_map/all_to_all | solution.py:26
  41.7 0.2 multiply_add_fusion
  41.9 0.6 fusion.8
  42.7 0.7 broadcast_in_dim.13
  43.4 6.0 %all-to-all-start.1 = ((bf16[32,8,256]{2,1,0:T(8,128)(2,1)}), bf16[32,8,256]{2,1,0:T(8,128)(2,1)S(1)}, u32[]{:S(2)}, u32[]{:S(2)}) async-start(bf16[32,8,256]{2,1,0:T(8,128)(2,1)} %broadcast_in_dim.13), calls=%async_computation.1 | async-start | bytes 262144 | tf_op jit(solution)/shard_map/all_to_all | solution.py:44
  49.4 0.7 copy-done.13
  50.3 4.3 %scatter_custom_fusion = s32[2048]{0:T(1024)S(1)} fusion(s32[1024]{0:T(1024)S(1)} %bitcast.88, s32[1024]{0:T(1024)S(1)} %add_select_fusion, s32[]{:T(128)} %constant.47.clone.1), kind=kCustom, calls=%fused_computation.117 | custom fusion | bytes 8196 | tf_op jit(solution)/shard_map/scatter | solution.py:128
  54.6 4.3 %all-to-all-done.1 = bf16[32,8,256]{2,1,0:T(8,128)(2,1)S(1)} async-done(((bf16[32,8,256]{2,1,0:T(8,128)(2,1)}), bf16[32,8,256]{2,1,0:T(8,128)(2,1)S(1)}, u32[]{:S(2)}, u32[]{:S(2)}) %all-to-all-start.1) | async-done | bytes 131104 | tf_op jit(solution)/shard_map/all_to_all | solution.py:44
  59.0 22.2 %all-gather = bf16[4096,64]{0,1:T(8,128)(2,1)S(1)} all-gather(bf16[256,64]{0,1:T(8,128)(2,1)S(1)} %convolution_convert_fusion.2), channel_id=2, replica_groups=mesh['ep'=32,'tp'=16] {'tp'}, dimensions={0}, use_global_device_ids=true | all-gather | bytes 557056 | tf_op jit(solution)/shard_map/all_gather | solution.py:61
  81.3 0.3 copy.98
  81.7 0.2 bitcast_reduce_fusion.1
  82.1 0.6 copy-done.10
  83.0 0.5 copy-done.18
  83.7 6.2 %gather_fusion = bf16[2048,64]{1,0:T(8,128)(2,1)S(1)} fusion(bf16[257,64]{1,0:T(8,128)(2,1)S(1)} %concatenate.47, s32[2048]{0:T(1024)S(1)} %fusion.55), kind=kCustom, calls=%fused_computation | custom fusion | bytes 532480 | tf_op jit(solution)/shard_map/gather | solution.py:206
  89.8 1.1 reshape.350
  90.9 4.1 %all-to-all-start.2 = ((bf16[32,2,2048]{2,1,0:T(2,128)(2,1)}), bf16[32,2,2048]{2,1,0:T(2,128)(2,1)S(1)}, u32[]{:S(2)}, u32[]{:S(2)}) async-start(bf16[32,2,2048]{2,1,0:T(2,128)(2,1)} %reshape.350), calls=%async_computation.2 | async-start | bytes 524288 | tf_op jit(solution)/shard_map/all_to_all | solution.py:207
  95.0 1.1 all_to_all.48
  96.1 10.5 %all-to-all-done.2 = bf16[32,2,2048]{2,1,0:T(2,128)(2,1)S(1)} async-done(((bf16[32,2,2048]{2,1,0:T(2,128)(2,1)}), bf16[32,2,2048]{2,1,0:T(2,128)(2,1)S(1)}, u32[]{:S(2)}, u32[]{:S(2)}) %all-to-all-start.2) | async-done | bytes 262176 | tf_op jit(solution)/shard_map/all_to_all | solution.py:207
  106.6 4.5 %all-to-all-start.6 = ((f32[32,1,2064]{2,1,0:T(1,128)}), f32[32,1,2064]{2,1,0:T(1,128)S(1)}, u32[]{:S(2)}, u32[]{:S(2)}) async-start(f32[32,1,2064]{2,1,0:T(1,128)} %all_to_all.48), calls=%async_computation.6 | async-start | bytes 557056 | tf_op jit(solution)/shard_map/all_to_all | solution.py:26
  111.2 0.4 reshape.351
  111.6 0.3 fusion.7
  111.9 0.3 copy.87
  112.2 0.4 convert_element_type.104
  112.7 0.6 copy-done.3
  113.3 0.2 fusion
  113.5 0.8 copy-done.4
  114.3 0.4 convolution_convert_fusion
  114.7 0.8 reshape.301
  115.5 6.4 %all-to-all-done.6 = f32[32,1,2064]{2,1,0:T(1,128)S(1)} async-done(((f32[32,1,2064]{2,1,0:T(1,128)}), f32[32,1,2064]{2,1,0:T(1,128)S(1)}, u32[]{:S(2)}, u32[]{:S(2)}) %all-to-all-start.6) | async-done | bytes 264224 | tf_op jit(solution)/shard_map/all_to_all | solution.py:26
  121.9 7.8 %all-to-all-start.3 = ((bf16[16,4,2048]{2,1,0:T(4,128)(2,1)}), bf16[16,4,2048]{2,1,0:T(4,128)(2,1)S(1)}, u32[]{:S(2)}, u32[]{:S(2)}) async-start(bf16[16,4,2048]{2,1,0:T(4,128)(2,1)} %reshape.301), calls=%async_computation.3 | async-start | bytes 524288 | tf_op jit(solution)/shard_map/all_to_all | solution.py:67
  129.7 0.2 reduce_sum.114
  129.9 11.4 %all-to-all-done.3 = bf16[16,4,2048]{2,1,0:T(4,128)(2,1)S(1)} async-done(((bf16[16,4,2048]{2,1,0:T(4,128)(2,1)}), bf16[16,4,2048]{2,1,0:T(4,128)(2,1)S(1)}, u32[]{:S(2)}, u32[]{:S(2)}) %all-to-all-start.3) | async-done | bytes 262176 | tf_op jit(solution)/shard_map/all_to_all | solution.py:67
  141.3 0.8 broadcast_in_dim.18
  142.1 3.9 %all-to-all-start.7 = ((f32[32,1,2064]{2,1,0:T(1,128)}), f32[32,1,2064]{2,1,0:T(1,128)S(1)}, u32[]{:S(2)}, u32[]{:S(2)}) async-start(f32[32,1,2064]{2,1,0:T(1,128)} %broadcast_in_dim.18), calls=%async_computation.7 | async-start | bytes 557056 | tf_op jit(solution)/shard_map/all_to_all | solution.py:44
  146.1 13.0 %all-to-all-done.7 = f32[32,1,2064]{2,1,0:T(1,128)S(1)} async-done(((f32[32,1,2064]{2,1,0:T(1,128)}), f32[32,1,2064]{2,1,0:T(1,128)S(1)}, u32[]{:S(2)}, u32[]{:S(2)}) %all-to-all-start.7) | async-done | bytes 264224 | tf_op jit(solution)/shard_map/all_to_all | solution.py:44
  159.1 0.8 broadcast_in_dim.16
  159.9 3.9 %all-to-all-start.4 = ((bf16[16,4,2048]{2,1,0:T(4,128)(2,1)}), bf16[16,4,2048]{2,1,0:T(4,128)(2,1)S(1)}, u32[]{:S(2)}, u32[]{:S(2)}) async-start(bf16[16,4,2048]{2,1,0:T(4,128)(2,1)} %broadcast_in_dim.16), calls=%async_computation.4 | async-start | bytes 524288 | tf_op jit(solution)/shard_map/all_to_all | solution.py:44
  164.0 0.7 reduce.7
  164.6 0.2 slice.52
  164.9 0.2 reshape.304
  165.1 10.5 %all-to-all-done.4 = bf16[16,4,2048]{2,1,0:T(4,128)(2,1)S(1)} async-done(((bf16[16,4,2048]{2,1,0:T(4,128)(2,1)}), bf16[16,4,2048]{2,1,0:T(4,128)(2,1)S(1)}, u32[]{:S(2)}, u32[]{:S(2)}) %all-to-all-start.4) | async-done | bytes 262176 | tf_op jit(solution)/shard_map/all_to_all | solution.py:44
  175.7 0.7 copy.88
  176.4 0.5 broadcast.245
  176.9 11.5 %reduce.10 = bf16[2048,64]{1,0:T(8,128)(2,1)S(1)} reduce(bf16[2048,1,64]{2,1,0:T(2,128)(2,1)S(1)} %bitcast.80, bf16[]{:T(256)} %broadcast.245), dimensions={1}, to_apply=%bitcast.71.reduce_sub_computation | reduce | bytes 524290
  188.5 1.1 reshape.352
  189.6 4.4 %all-to-all-start.5 = ((bf16[32,2,2048]{2,1,0:T(2,128)(2,1)}), bf16[32,2,2048]{2,1,0:T(2,128)(2,1)S(1)}, u32[]{:S(2)}, u32[]{:S(2)}) async-start(bf16[32,2,2048]{2,1,0:T(2,128)(2,1)} %reshape.352), calls=%async_computation.5 | async-start | bytes 524288 | tf_op jit(solution)/shard_map/all_to_all | solution.py:225
  194.0 0.2 convolution_convert_fusion.1
  194.2 15.9 %all-gather.1 = bf16[4096,64]{0,1:T(8,128)(2,1)S(1)} all-gather(bf16[256,64]{0,1:T(8,128)(2,1)S(1)} %convolution_convert_fusion.1), channel_id=3, replica_groups=mesh['ep'=32,'tp'=16] {'tp'}, dimensions={0}, use_global_device_ids=true | all-gather | bytes 557056 | tf_op jit(solution)/shard_map/all_gather | solution.py:61
  210.2 0.3 copy.100
  210.5 0.2 bitcast_reduce_fusion
  210.8 0.6 reshape.353
  211.4 0.6 copy.89
  212.0 0.5 all_to_all.46
  212.5 0.2 copy.90
  212.8 3.2 %gather_fusion.1 = bf16[1024,64]{1,0:T(8,128)(2,1)S(1)} fusion(bf16[2048,64]{1,0:T(8,128)(2,1)S(1)} %bitcast.78, s32[1024]{0:T(1024)S(1)} %broadcast_clamp_fusion), kind=kCustom, calls=%fused_computation.1 | custom fusion | bytes 266240 | tf_op jit(solution)/shard_map/gather | solution.py:226
  216.0 0.4 fusion.12
  216.5 0.7 copy.94
  (82 shorter events, 3.6 us)
Async XLA Ops:
  0.6 112.9 %copy-start = (bf16[1,128,2048]{2,1,0:T(8,128)(2,1)S(1)}, bf16[1,128,2048]{2,1,0:T(8,128)(2,1)}, u32[]{:S(2)}) copy-start(bf16[1,128,2048]{2,1,0:T(8,128)(2,1)} %param.33) | copy-start | bytes 1572868
  1.7 0.8 copy-start.5
  1.7 0.8 copy-start.6
  1.7 0.8 copy-start.8
  1.7 0.7 copy-start.9
  1.7 0.7 copy-start.15
  3.7 13.9 %copy-start.17 = (s32[8]{0:T(128)S(1)}, s32[8]{0:T(128)}, u32[]{:S(2)}) copy-start(s32[8]{0:T(128)} %param.29) | copy-start | bytes 100
  3.7 13.9 %copy-start.12 = (s32[256,4]{0,1:T(4,128)S(1)}, s32[256,4]{0,1:T(4,128)}, u32[]{:S(2)}) copy-start(s32[256,4]{0,1:T(4,128)} %param.34) | copy-start | bytes 12292
  3.7 37.4 %all-to-all-start = ((f32[32,8,769]{2,1,0:T(8,128)}), f32[32,8,769]{2,1,0:T(8,128)S(1)}, u32[]{:S(2)}, u32[]{:S(2)}) async-start(f32[32,8,769]{2,1,0:T(8,128)} %pad_maximum_fusion), calls=%async_computation | async-start | bytes 1835008 | tf_op jit(solution)/shard_map/all_to_all | solution.py:26
  17.6 24.1 %copy-start.2 = (f32[8,1,128,256]{3,2,1,0:T(8,128)S(1)}, f32[8,1,128,256]{3,2,1,0:T(8,128)}, u32[]{:S(2)}) copy-start(f32[8,1,128,256]{3,2,1,0:T(8,128)} %param.28) | copy-start | bytes 3145732
  41.9 39.3 %copy-start.1 = (f32[8,1,128,256]{3,2,1,0:T(8,128)}, f32[8,1,128,256]{3,2,1,0:T(8,128)S(1)}, u32[]{:S(2)}) copy-start(f32[8,1,128,256]{3,2,1,0:T(8,128)S(1)} %multiply_add_fusion) | copy-start | bytes 3145732
  43.4 15.4 %all-to-all-start.1 = ((bf16[32,8,256]{2,1,0:T(8,128)(2,1)}), bf16[32,8,256]{2,1,0:T(8,128)(2,1)S(1)}, u32[]{:S(2)}, u32[]{:S(2)}) async-start(bf16[32,8,256]{2,1,0:T(8,128)(2,1)} %broadcast_in_dim.13), calls=%async_computation.1 | async-start | bytes 262144 | tf_op jit(solution)/shard_map/all_to_all | solution.py:44
  49.4 0.7 copy-start.13
  49.4 9.4 %copy-start.7 = (bf16[256,64]{0,1:T(8,128)(2,1)S(1)}, bf16[256,64]{0,1:T(8,128)(2,1)}, u32[]{:S(2)}) copy-start(bf16[256,64]{0,1:T(8,128)(2,1)} %param.27) | copy-start | bytes 98308
  81.9 0.7 copy-start.10
  81.9 0.7 copy-start.11
  82.8 0.7 copy-start.18
  90.9 15.7 %all-to-all-start.2 = ((bf16[32,2,2048]{2,1,0:T(2,128)(2,1)}), bf16[32,2,2048]{2,1,0:T(2,128)(2,1)S(1)}, u32[]{:S(2)}, u32[]{:S(2)}) async-start(bf16[32,2,2048]{2,1,0:T(2,128)(2,1)} %reshape.350), calls=%async_computation.2 | async-start | bytes 524288 | tf_op jit(solution)/shard_map/all_to_all | solution.py:207
  106.6 15.3 %all-to-all-start.6 = ((f32[32,1,2064]{2,1,0:T(1,128)}), f32[32,1,2064]{2,1,0:T(1,128)S(1)}, u32[]{:S(2)}, u32[]{:S(2)}) async-start(f32[32,1,2064]{2,1,0:T(1,128)} %all_to_all.48), calls=%async_computation.6 | async-start | bytes 557056 | tf_op jit(solution)/shard_map/all_to_all | solution.py:26
  112.2 1.0 copy-start.3
  113.3 1.0 copy-start.4
  121.9 19.4 %all-to-all-start.3 = ((bf16[16,4,2048]{2,1,0:T(4,128)(2,1)}), bf16[16,4,2048]{2,1,0:T(4,128)(2,1)S(1)}, u32[]{:S(2)}, u32[]{:S(2)}) async-start(bf16[16,4,2048]{2,1,0:T(4,128)(2,1)} %reshape.301), calls=%async_computation.3 | async-start | bytes 524288 | tf_op jit(solution)/shard_map/all_to_all | solution.py:67
  142.1 17.0 %all-to-all-start.7 = ((f32[32,1,2064]{2,1,0:T(1,128)}), f32[32,1,2064]{2,1,0:T(1,128)S(1)}, u32[]{:S(2)}, u32[]{:S(2)}) async-start(f32[32,1,2064]{2,1,0:T(1,128)} %broadcast_in_dim.18), calls=%async_computation.7 | async-start | bytes 557056 | tf_op jit(solution)/shard_map/all_to_all | solution.py:44
  159.9 3.9 %copy-start.14 = (f32[256,4]{0,1:T(4,128)S(1)}, f32[256,4]{0,1:T(4,128)}, u32[]{:S(2)}) copy-start(f32[256,4]{0,1:T(4,128)} %param.35) | copy-start | bytes 12292
  159.9 15.7 %all-to-all-start.4 = ((bf16[16,4,2048]{2,1,0:T(4,128)(2,1)}), bf16[16,4,2048]{2,1,0:T(4,128)(2,1)S(1)}, u32[]{:S(2)}, u32[]{:S(2)}) async-start(bf16[16,4,2048]{2,1,0:T(4,128)(2,1)} %broadcast_in_dim.16), calls=%async_computation.4 | async-start | bytes 524288 | tf_op jit(solution)/shard_map/all_to_all | solution.py:44
  189.6 4.4 %copy-start.16 = (bf16[128,64]{0,1:T(8,128)(2,1)S(1)}, bf16[128,64]{0,1:T(8,128)(2,1)}, u32[]{:S(2)}) copy-start(bf16[128,64]{0,1:T(8,128)(2,1)} %param.38) | copy-start | bytes 49156
  189.6 21.2 %all-to-all-start.5 = ((bf16[32,2,2048]{2,1,0:T(2,128)(2,1)}), bf16[32,2,2048]{2,1,0:T(2,128)(2,1)S(1)}, u32[]{:S(2)}, u32[]{:S(2)}) async-start(bf16[32,2,2048]{2,1,0:T(2,128)(2,1)} %reshape.352), calls=%async_computation.5 | async-start | bytes 524288 | tf_op jit(solution)/shard_map/all_to_all | solution.py:225
where the time goes:
time: 218 us; the launch traced here: 217 us
  waiting for transfers between devices  77.5 us (36%)
  starting transfers between devices  48.3 us (22%)
  blocking collectives  38.1 us (17%)
  local copies, waits for them, and re-layouts  32.7 us (15%)
  other arithmetic  17.1 us (8%)
    all_gather x2, blocking collectives, total_of_pieces(): pieces = lax.all_gather(value, axis).astype(jnp.float32)  38.1 us
    all_to_all x2, waiting for transfers between devices, summed_on_arrival(): lax.all_to_all(pieces, axis, split_axis=0, concat_axis=0, tiled=True)  27.8 us
    all_to_all x3, waiting for transfers between devices, from_everyone(): lax.all_to_all(jnp.broadcast_to(value[None], (peers, *value.shape)), axis...  27.7 us
    all_to_all x2, starting transfers between devices, summed_on_arrival(): lax.all_to_all(pieces, axis, split_axis=0, concat_axis=0, tiled=True)  18.4 us
    all_to_all x3, starting transfers between devices, from_everyone(): lax.all_to_all(jnp.broadcast_to(value[None], (peers, *value.shape)), axis...  13.7 us
    unnamed x1, other arithmetic  11.5 us
    all_to_all x1, waiting for transfers between devices, sum_at_owner(): lax.all_to_all(pieces, axis, split_axis=0, concat_axis=0, tiled=True)  11.4 us
    all_to_all x1, waiting for transfers between devices, per_device(): lax.all_to_all(outgoing, 'ep', split_axis=0, concat_axis=2, tiled=True)[0]  10.5 us
  transfers between devices with their start and end apart: 8, of which 7 were waited for; matrix products, arithmetic and copies ran while one was open for 5% of the time, Pallas kernels for 0%

commit v1 on v0

v1 whole, which is shorter than its diff:
```python
import functools

import jax
import jax.numpy as jnp
from jax import lax
from jax.experimental import pallas as pl
from jax.experimental.pallas import tpu as pltpu
from jax.sharding import Mesh, PartitionSpec as P

D = 2048
KEY_DIM = 128
VAL_DIM = 256
EPS = 1e-06
LIMIT = 7.0
ALPHA = 1.702
F32 = jnp.float32
BF16 = jnp.bfloat16
EP = ("z", "x")


def mm(a, b):
    return jnp.dot(a, b, preferred_element_type=F32)


def two_part(v):
    high = v.astype(BF16).astype(F32)
    return high, v - high


def lane_of(shape):
    return lax.broadcasted_iota(jnp.int32, shape, len(shape) - 1)


def project_body(res_ref, gain_ref, q_ref, k_ref, v_ref, g_ref, out_ref):
    rows = res_ref[...].astype(F32)
    normed = (rows * gain_ref[...]).astype(BF16)
    at = 0
    for ref in (q_ref, k_ref, v_ref, g_ref):
        width = ref.shape[1]
        part = mm(normed, ref[...])
        out_ref[:, :, at : at + width] = part.reshape(32, 8, width).astype(BF16)
        at += width
    high, low = two_part(jnp.sum(rows * rows, axis=1, keepdims=True))
    lane = lane_of((256, 128))
    stats = jnp.where(lane == 0, high, jnp.where(lane == 1, low, 0.0))
    out_ref[:, :, at : at + 128] = stats.reshape(32, 8, 128).astype(BF16)


def dispatch_body(am_ref, sel_ref, gain_ref, mix_ref, dw_ref, out_ref):
    am = am_ref[...]
    lane = lane_of(am.shape)
    left = lane < 64
    amf = am.astype(F32)
    stacked = jnp.concatenate([jnp.where(left, amf, 0.0), jnp.where(left, 0.0, amf)], axis=0)
    sent = mm(sel_ref[...], stacked.astype(BF16))
    out_ref[:, 0:32, :] = sent.reshape(32, 32, 128).astype(BF16)
    normed = (stacked * gain_ref[...]).astype(BF16)
    both = mm(normed, dw_ref[...])
    out_ref[:, 32:40, :] = both[:, :128].reshape(32, 8, 128).astype(BF16)
    out_ref[:, 40:48, :] = both[:, 128:].reshape(32, 8, 128).astype(BF16)
    sq_high, sq_low = two_part(jnp.sum(stacked * stacked, axis=1, keepdims=True))
    mx_high, mx_low = two_part(
        jnp.sum(normed.astype(F32) * mix_ref[...], axis=1, keepdims=True)
    )
    lane2 = lane_of((256, 128))
    stats = jnp.where(
        lane2 == 0,
        sq_high,
        jnp.where(
            lane2 == 1, sq_low, jnp.where(lane2 == 2, mx_high, jnp.where(lane2 == 3, mx_low, 0.0))
        ),
    )
    out_ref[:, 48:56, :] = stats.reshape(32, 8, 128).astype(BF16)


def expert_body(arr_ref, gain_ref, eg_ref, eu_ref, ed_ref, weight_ref, out_ref, zn_ref):
    tail = jnp.sum(arr_ref[:, 32:56, :].astype(F32), axis=0)
    stats = tail[16:24]
    scale = lax.rsqrt((stats[:, 0:1] + stats[:, 1:2]) / D + EPS)
    mix = jax.nn.sigmoid(scale * (stats[:, 2:3] + stats[:, 3:4]))
    act = jax.nn.silu(tail[0:8] * scale) * (tail[8:16] * scale) * mix
    out_ref[:, 32:40, :] = jnp.broadcast_to(act[None], (32, 8, 128)).astype(BF16)
    left = lane_of((32, 128)) < 64
    squares = jnp.zeros((64, 128), F32)
    for p in range(16):
        a = arr_ref[2 * p, 0:32, :].astype(F32)
        b = arr_ref[2 * p + 1, 0:32, :].astype(F32)
        z = jnp.concatenate(
            [
                jnp.where(left, a, pltpu.roll(b, 64, 1)),
                jnp.where(left, pltpu.roll(a, 64, 1), b),
            ],
            axis=0,
        )
        squares = squares + z * z
        zn_ref[:, 128 * p : 128 * p + 128] = (
            z * gain_ref[:, 128 * p : 128 * p + 128]
        ).astype(BF16)
    norm = lax.rsqrt(jnp.sum(squares, axis=1, keepdims=True) / D + EPS)
    zn = zn_ref[...]
    gate = jnp.minimum(mm(zn, eg_ref[...]) * norm, LIMIT)
    up = jnp.clip(mm(zn, eu_ref[...]) * norm, -LIMIT, LIMIT)
    hidden = ((up + 1.0) * gate * jax.nn.sigmoid(ALPHA * gate)).astype(BF16)
    weight = weight_ref[...]
    for p in range(16):
        o = mm(hidden, ed_ref[:, 128 * p : 128 * p + 128]) * weight
        low, high = o[0:32], o[32:64]
        out_ref[2 * p, 0:32, :] = jnp.where(left, low, pltpu.roll(high, 64, 1)).astype(BF16)
        out_ref[2 * p + 1, 0:32, :] = jnp.where(left, pltpu.roll(low, 64, 1), high).astype(BF16)


def collect_body(arr_ref, low_ref, high_ref, dd_ref, out_ref):
    slots = arr_ref[:, 0:32, :].reshape(1024, 128)
    left = lane_of((128, 128)) < 64
    routed = jnp.where(left, mm(low_ref[...], slots), mm(high_ref[...], slots))
    act = arr_ref[:, 32:40, :].astype(F32).reshape(256, 128).astype(BF16)
    dense = mm(act[:128], dd_ref[0:128]) + mm(act[128:], dd_ref[128:256])
    out_ref[...] = (routed + dense).astype(BF16)


def call(body, out_shape, *args, scratch=()):
    return pl.pallas_call(
        body,
        out_shape=jax.ShapeDtypeStruct(out_shape, BF16),
        in_specs=[pl.BlockSpec(memory_space=pltpu.VMEM)] * len(args),
        out_specs=pl.BlockSpec(memory_space=pltpu.VMEM),
        scratch_shapes=list(scratch),
        name=body.__name__,
    )(*args)


def exchange(pieces, axes):
    return lax.all_to_all(pieces, axes, 0, 0, tiled=True)


def from_everyone(value, axes):
    peers = lax.axis_size(axes)
    return exchange(jnp.broadcast_to(value[None], (peers, *value.shape)), axes)


def own_half(value, core):
    rows = value.shape[0] // 2
    return lax.dynamic_slice_in_dim(value, core * rows, rows, 0)


def half_sum(partial, core):
    both = lax.all_gather(partial, "c")
    mine = lax.dynamic_slice_in_dim(both, core * 64, 64, 1).astype(F32)
    pair = (mine[0] + mine[1]).astype(BF16)
    return jnp.sum(from_everyone(pair, ("y",)).astype(F32), axis=0)


def packed(value):
    rows = value.shape[0] // 2
    return jnp.concatenate([value[:rows], value[rows:]], axis=1)


def block_pair(w):
    zero = jnp.zeros_like(w)
    return jnp.concatenate(
        [jnp.concatenate([w, zero], axis=1), jnp.concatenate([zero, w], axis=1)], axis=0
    )


def rotate_half(vectors, cosine, sine):
    a = vectors[:, :64]
    b = vectors[:, 64:]
    return jnp.concatenate([a * cosine - b * sine, b * cosine + a * sine], axis=1)


def routing(route_ids, route_weight, own):
    rows = route_ids.shape[0]
    names = jnp.arange(32, dtype=jnp.int32)
    hit = route_ids[:, :, None] == names[None, None, :]
    named = jnp.any(hit, axis=1)
    weight = jnp.sum(jnp.where(hit, route_weight[:, :, None], 0.0), axis=1)
    r = lax.broadcasted_iota(jnp.int32, (rows, rows), 0)
    q = lax.broadcasted_iota(jnp.int32, (rows, rows), 1)
    before = ((r // 8 == q // 8) & (q < r)).astype(BF16)
    earlier = mm(before, named.astype(BF16))
    group = lax.broadcasted_iota(jnp.int32, (rows, 1), 0) // 8
    place = ((group % 16) * 2).astype(F32) + earlier
    place = jnp.where(named, place, 64.0).astype(BF16)
    x = lax.broadcasted_iota(jnp.int32, (32, 1024), 0)
    slot = lax.broadcasted_iota(jnp.int32, (32, 1024), 1)
    spread = (slot // 32 == x).astype(BF16)
    wide = mm(place, spread)
    step = (lax.broadcasted_iota(jnp.int32, (1, 1024), 1) % 32).astype(F32)
    back = (wide == step).astype(BF16)
    tall = lax.dot_general(spread, place, (((0,), (1,)), ((), ())), preferred_element_type=F32)
    down = (lax.broadcasted_iota(jnp.int32, (1024, 1), 0) % 32).astype(F32)
    forth = (tall == down).astype(BF16)
    mine = lax.dynamic_slice_in_dim(forth, own * 32, 32, 0).astype(F32)
    own_weight = lax.dynamic_slice_in_dim(weight, own, 1, 1).reshape(1, rows)
    scaled = mine * own_weight
    slot_weight = jnp.concatenate(
        [
            jnp.sum(scaled[:, :128], axis=1, keepdims=True),
            jnp.sum(scaled[:, 128:], axis=1, keepdims=True),
        ],
        axis=0,
    )
    return forth, back[:128], back[128:], jnp.broadcast_to(slot_weight, (64, 128))


def per_device(
    residual,
    norm_gain,
    query_weight,
    key_weight,
    value_weight,
    gate_weight,
    out_weight,
    prior_state,
    lengths,
    ffn_gain,
    expert_gate,
    expert_up,
    expert_down,
    route_ids,
    route_weight,
    dense_gate,
    dense_up,
    dense_down,
    mix_vector,
):
    own = lax.axis_index(EP)
    core = lax.axis_index("c")
    head = lax.axis_index("y") * 2 + core
    terms = call(
        project_body,
        (32, 8, 896),
        residual,
        norm_gain[None, :],
        query_weight,
        key_weight,
        value_weight,
        gate_weight,
    )
    arrived = exchange(terms, EP)

    forth, back_low, back_high, slot_weight = routing(route_ids, route_weight, own)
    out_pair = block_pair(out_weight)
    down_pair = block_pair(dense_down)
    gain_here = lax.dynamic_slice_in_dim(ffn_gain, own * 64, 64, 0)
    gain_pair = jnp.concatenate([gain_here, gain_here])[None, :]
    mix_pair = jnp.concatenate([mix_vector, mix_vector]).astype(F32)[None, :]
    dense_in = jnp.concatenate([dense_gate, dense_up], axis=1)
    dense_in = jnp.concatenate([dense_in, dense_in], axis=0)
    residual_half = own_half(packed(residual), core).astype(F32)
    inverse = 1.0 / 10000.0 ** jnp.linspace(0.0, 1.0, 64, dtype=F32)
    angles = lengths.astype(F32)[:, None] * inverse[None, :]
    cosine = jnp.cos(angles)
    sine = jnp.sin(angles)

    summed = jnp.sum(arrived.astype(F32), axis=0)
    row_scale = lax.rsqrt((summed[:, 768:769] + summed[:, 769:770]) / D + EPS)
    projected = summed[:, :768] * row_scale
    query_rot = rotate_half(projected[:, :128], cosine, sine)
    key_rot = rotate_half(projected[:, 128:256], cosine, sine) * KEY_DIM ** (-0.5)
    values = projected[:, 256:512]
    gate_pre = projected[:, 512:768]
    decay = 1.0 - jnp.exp2(-1.0 - 0.5 * head.astype(F32))
    new_state = decay * prior_state + key_rot[:, None, :, None] * values[:, None, None, :]
    read = jnp.sum(query_rot[:, :, None] * new_state[:, 0], axis=1)
    normed = read * lax.rsqrt(jnp.mean(read * read, axis=-1, keepdims=True) + EPS)
    gated = (normed * jax.nn.silu(gate_pre)).astype(BF16)

    heads = from_everyone(gated, EP).reshape(256, VAL_DIM)
    attn = mm(packed(heads), out_pair).astype(BF16)
    after_half = (residual_half + half_sum(attn, core)).astype(BF16)
    after = lax.all_gather(after_half, "c", tiled=True)

    sent = call(dispatch_body, (32, 56, 128), after, forth, gain_pair, mix_pair, dense_in)
    inbox = exchange(sent, EP)
    made = call(
        expert_body,
        (32, 40, 128),
        inbox,
        ffn_gain[None, :],
        expert_gate[0],
        expert_up[0],
        expert_down[0],
        slot_weight,
        scratch=(pltpu.VMEM((64, D), BF16),),
    )
    returned = exchange(made, EP)
    branch = call(collect_body, (128, 128), returned, back_low, back_high, down_pair)
    out_half = (after_half.astype(F32) + half_sum(branch, core)).astype(BF16)
    out = lax.all_gather(out_half, "c", tiled=True)
    layer_out = jnp.concatenate([out[:, :64], out[:, 64:]], axis=0)
    return layer_out, new_state


def solution(mesh):
    fine = Mesh(mesh.devices.reshape(8, 4, 8, 2), ("z", "x", "y", "c"))
    tp = ("y", "c")
    placed = (
        P(None, EP),
        P(EP),
        P(EP, tp),
        P(EP, tp),
        P(EP, tp),
        P(EP, tp),
        P(tp, EP),
        P(EP, tp, None, None),
        P(EP),
        P(),
        P(EP, None, tp),
        P(EP, None, tp),
        P(EP, tp, None),
        P(),
        P(),
        P(EP, tp),
        P(EP, tp),
        P(tp, EP),
        P(EP),
    )
    return jax.shard_map(
        per_device,
        mesh=fine,
        in_specs=placed,
        out_specs=(P(None, EP), P(EP, tp, None, None)),
        check_vma=False,
    )
```

time: 218 us -> 140 us (0.64)
  waiting for transfers between devices: 77.5 us -> 50.4 us
  local copies, waits for them, and re-layouts: 32.7 us -> 8.28 us
  starting transfers between devices: 48.3 us -> 35.5 us
  other arithmetic: 17.1 us -> 5.81 us
  blocking collectives: 38.1 us -> 26.9 us
  Pallas kernels: 0 us -> 9.1 us
    all_to_all x8 -> x5, waiting for transfers between devices: 77.5 us -> 50.4 us  [exchange(): return lax.all_to_all(pieces, axes, 0, 0, tiled=True)]
    all_gather x2 -> x4, blocking collectives: 38.1 us -> 16.1 us  [the longest x2 9.29 us: half_sum(): both = lax.all_gather(partial, 'c')]
    all_to_all x8 -> x5, starting transfers between devices: 48.3 us -> 35.5 us  [exchange(): return lax.all_to_all(pieces, axes, 0, 0, tiled=True)]
    unnamed x1 -> x0, other arithmetic: 11.5 us -> none
    all_to_all x0 -> x1, blocking collectives: none -> 10.8 us  [exchange(): return lax.all_to_all(pieces, axes, 0, 0, tiled=True)]
    gather x2 -> x0, local copies, waits for them, and re-layouts: 9.39 us -> none  [the longest x1 6.18 us: per_device(): outgoing = padded[slot_source].reshape(ep_count, slot_count, local_width)]
    pallas_call x0 -> x4, Pallas kernels: none -> 9.1 us  [call(): pl.pallas_call(body, out_shape=jax.ShapeDtypeStruct(out_shape, BF16), in_...]
    unnamed x50 -> x27, local copies, waits for them, and re-layouts: 10.1 us -> 4.45 us
  transfers between devices with their start and end apart: 8 -> 5, of which waited for: 7 -> 5; matrix products, arithmetic and copies ran while one was open for 5% -> 5% of each run, Pallas kernels for 0% -> 0%
where the time goes in v1:
time: 140 us; the launch traced here: 139 us
  waiting for transfers between devices  50.4 us (36%)
  starting transfers between devices  35.5 us (25%)
  blocking collectives  26.9 us (19%)
  Pallas kernels  9.1 us (6%)
  local copies, waits for them, and re-layouts  8.28 us (6%)
  other arithmetic  5.81 us (4%)
  matrix products  1.96 us (1%)
    all_to_all x5, waiting for transfers between devices, exchange(): return lax.all_to_all(pieces, axes, 0, 0, tiled=True)  50.4 us
    all_to_all x5, starting transfers between devices, exchange(): return lax.all_to_all(pieces, axes, 0, 0, tiled=True)  35.5 us
    all_to_all x1, blocking collectives, exchange(): return lax.all_to_all(pieces, axes, 0, 0, tiled=True)  10.8 us
    all_gather x2, blocking collectives, half_sum(): both = lax.all_gather(partial, 'c')  9.29 us
    pallas_call x4, Pallas kernels, call(): pl.pallas_call(body, out_shape=jax.ShapeDtypeStruct(out_shape, BF16), in_...  9.1 us
    unnamed x27, local copies, waits for them, and re-layouts  4.45 us
    all_gather x1, blocking collectives, per_device(): after = lax.all_gather(after_half, 'c', tiled=True)  3.69 us
    all_gather x1, blocking collectives, per_device(): out = lax.all_gather(out_half, 'c', tiled=True)  3.11 us
  transfers between devices with their start and end apart: 5, of which 5 were waited for; matrix products, arithmetic and copies ran while one was open for 5% of the time, Pallas kernels for 0%

profile of v1, /device:TPU:1, one launch (start us, length us, event | category | flops | bytes accessed | tf_op | source)
XLA Modules:
  0.0 138.8 jit_solution(13703772546974962690)
XLA Ops:
  0.6 1.5 %copy.61.res_ref = bf16[256,64]{1,0:T(8,128)(2,1)} copy(bf16[256,64]{0,1:T(8,128)(2,1)} %param.19) | data formatting | bytes 65536 | tf_op args[0]
  2.1 0.0 copy-start.10
  2.1 1.9 %project_body.1 = bf16[32,8,896]{2,1,0:T(8,128)(2,1)} custom-call(bf16[256,64]{1,0:T(8,128)(2,1)} %copy.61.res_ref, f32[1,64]{1,0:T(1,128)} %bitcast.39, bf16[64,128]{1,0:T(8,128)(2,1)} %q_ref.1, bf16[64,128]{1,0:T(8,128)(2,1)} %k_ref.1, bf16[64,256]{1,0:T(8,128)(2,1)} %v_ref.1, bf16[64,256]{1,0:T(8,128)(2,1)} %g_ref.1), custom_call_target="tpu_custom_call" | custom-call | tf_op jit(solution)/shard_map/project_body/pallas_call | solution.py:122
  4.1 13.8 %all-to-all-start = ((bf16[32,8,896]{2,1,0:T(8,128)(2,1)}), bf16[32,8,896]{2,1,0:T(8,128)(2,1)S(1)}, u32[]{:S(2)}, u32[]{:S(2)}) async-start(bf16[32,8,896]{2,1,0:T(8,128)(2,1)} %project_body.1), calls=%async_computation | async-start | bytes 917504 | tf_op jit(solution)/shard_map/all_to_all | solution.py:133
  18.0 0.0 copy-done.10
  18.0 0.8 dynamic_slice.20
  18.8 0.1 fusion.68
  18.9 0.0 copy-done.6
  18.9 0.0 copy-done.7
  18.9 0.0 copy-start.5
  18.9 0.6 maximum_maximum_fusion.dw_ref
  19.6 0.0 copy-done.5
  19.6 0.3 fusion.3
  19.9 12.4 %all-to-all-done = bf16[32,8,896]{2,1,0:T(8,128)(2,1)S(1)} async-done(((bf16[32,8,896]{2,1,0:T(8,128)(2,1)}), bf16[32,8,896]{2,1,0:T(8,128)(2,1)S(1)}, u32[]{:S(2)}, u32[]{:S(2)}) %all-to-all-start) | async-done | bytes 458784 | tf_op jit(solution)/shard_map/all_to_all | solution.py:133
  32.4 0.1 convert_reduce_fusion
  32.4 0.2 fusion.63
  32.6 0.1 slice_multiply_fusion
  32.7 0.1 fusion.56
  32.8 0.1 pad_maximum_fusion.1
  32.9 0.0 copy-done.2
  32.9 1.3 fusion.4
  34.2 0.1 multiply_reduce_fusion
  34.3 0.1 multiply_convert_fusion
  34.4 0.7 broadcast_in_dim.43
  35.1 5.7 %all-to-all-start.1 = ((bf16[32,8,256]{2,1,0:T(8,128)(2,1)}), bf16[32,8,256]{2,1,0:T(8,128)(2,1)S(1)}, u32[]{:S(2)}, u32[]{:S(2)}) async-start(bf16[32,8,256]{2,1,0:T(8,128)(2,1)} %broadcast_in_dim.43), calls=%async_computation.1 | async-start | bytes 262144 | tf_op jit(solution)/shard_map/all_to_all | solution.py:133
  40.8 0.6 maximum_bitcast_fusion.gain_ref
  41.4 1.2 fusion.sel_ref
  42.6 7.6 %all-to-all-done.1 = bf16[32,8,256]{2,1,0:T(8,128)(2,1)S(1)} async-done(((bf16[32,8,256]{2,1,0:T(8,128)(2,1)}), bf16[32,8,256]{2,1,0:T(8,128)(2,1)S(1)}, u32[]{:S(2)}, u32[]{:S(2)}) %all-to-all-start.1) | async-done | bytes 131104 | tf_op jit(solution)/shard_map/all_to_all | solution.py:133
  50.2 0.0 copy-done.9
  50.2 0.2 convolution_convert_fusion
  50.4 4.5 %all-gather = bf16[256,128]{1,0:T(8,128)(2,1)S(1)} all-gather(bf16[128,128]{1,0:T(8,128)(2,1)S(1)} %convolution_convert_fusion), channel_id=2, replica_groups=mesh['z'=8,'x'=4,'y'=8,'c'=2] {'c'}, dimensions={0}, use_global_device_ids=true | all-gather | bytes 98304 | tf_op jit(solution)/shard_map/all_gather | solution.py:147
  54.9 0.7 broadcast_in_dim.77
  55.6 7.0 %all-to-all-start.2 = ((bf16[8,64,128]{2,1,0:T(8,128)(2,1)}), bf16[8,64,128]{2,1,0:T(8,128)(2,1)S(1)}, u32[]{:S(2)}, u32[]{:S(2)}) async-start(bf16[8,64,128]{2,1,0:T(8,128)(2,1)} %broadcast_in_dim.77), calls=%async_computation.2 | async-start | bytes 262144 | tf_op jit(solution)/shard_map/all_to_all | solution.py:133
  62.5 0.7 copy-done.11
  63.2 0.6 maximum_convert_fusion.mix_ref
  63.8 0.0 copy-done.3
  63.8 6.7 %all-to-all-done.2 = bf16[8,64,128]{2,1,0:T(8,128)(2,1)S(1)} async-done(((bf16[8,64,128]{2,1,0:T(8,128)(2,1)}), bf16[8,64,128]{2,1,0:T(8,128)(2,1)S(1)}, u32[]{:S(2)}, u32[]{:S(2)}) %all-to-all-start.2) | async-done | bytes 131104 | tf_op jit(solution)/shard_map/all_to_all | solution.py:133
  70.5 0.1 add_convert_fusion.1
  70.6 3.7 %all_gather.20.am_ref = bf16[128,128]{1,0:T(8,128)(2,1)} all-gather(bf16[64,128]{1,0:T(8,128)(2,1)S(1)} %add_convert_fusion.1), channel_id=1, replica_groups=mesh['z'=8,'x'=4,'y'=8,'c'=2] {'c'}, dimensions={0}, use_global_device_ids=true | all-gather | bytes 49152 | tf_op jit(solution)/shard_map/all_gather | solution.py:272
  74.3 2.1 %dispatch_body.1 = bf16[32,56,128]{2,1,0:T(8,128)(2,1)} custom-call(bf16[128,128]{1,0:T(8,128)(2,1)} %all_gather.20.am_ref, bf16[1024,256]{1,0:T(8,128)(2,1)} %fusion.sel_ref, f32[1,128]{1,0:T(1,128)} %maximum_bitcast_fusion.gain_ref, f32[1,128]{1,0:T(1,128)} %maximum_convert_fusion.mix_ref, bf16[128,256]{1,0:T(8,128)(2,1)} %maximum_maximum_fusion.dw_ref), custom_call_target="tpu_custom_call" | custom-call | tf_op jit(solution)/shard_map/dispatch_body/pallas_call | solution.py:122
  76.4 3.9 %all-to-all-start.3 = ((bf16[32,56,128]{2,1,0:T(8,128)(2,1)}), bf16[32,56,128]{2,1,0:T(8,128)(2,1)S(1)}, u32[]{:S(2)}, u32[]{:S(2)}) async-start(bf16[32,56,128]{2,1,0:T(8,128)(2,1)} %dispatch_body.1), calls=%async_computation.3 | async-start | bytes 917504 | tf_op jit(solution)/shard_map/all_to_all | solution.py:133
  80.3 0.0 copy-start.8
  80.3 0.7 copy-done.8
  81.0 0.7 convert_multiply_fusion
  81.8 0.1 slice_reduce_fusion.1
  81.9 0.1 maximum_bitcast_fusion.1
  82.0 13.8 %all-to-all-done.3.arr_ref = bf16[32,56,128]{2,1,0:T(8,128)(2,1)S(1)} async-done(((bf16[32,56,128]{2,1,0:T(8,128)(2,1)}), bf16[32,56,128]{2,1,0:T(8,128)(2,1)S(1)}, u32[]{:S(2)}, u32[]{:S(2)}) %all-to-all-start.3) | async-done | bytes 458784 | tf_op jit(solution)/shard_map/all_to_all | solution.py:133
  95.8 0.8 broadcast_in_dim.86.weight_ref
  96.5 0.0 copy-done
  96.5 3.0 %expert_body.1 = bf16[32,40,128]{2,1,0:T(8,128)(2,1)} custom-call(bf16[32,56,128]{2,1,0:T(8,128)(2,1)} %copy-done, f32[1,2048]{1,0:T(1,128)} %bitcast.35, bf16[2048,128]{1,0:T(8,128)(2,1)} %bitcast.30, bf16[2048,128]{1,0:T(8,128)(2,1)} %bitcast.31, bf16[128,2048]{1,0:T(8,128)(2,1)} %bitcast.32, f32[64,128]{1,0:T(8,128)} %broadcast_in_dim.86.weight_ref), custom_call_target="tpu_custom_call" | custom-call | tf_op jit(solution)/shard_map/expert_body/pallas_call | solution.py:122
  99.5 5.1 %all-to-all-start.4 = ((bf16[32,40,128]{2,1,0:T(8,128)(2,1)}), bf16[32,40,128]{2,1,0:T(8,128)(2,1)S(1)}, u32[]{:S(2)}, u32[]{:S(2)}) async-start(bf16[32,40,128]{2,1,0:T(8,128)(2,1)} %expert_body.1), calls=%async_computation.4 | async-start | bytes 655360 | tf_op jit(solution)/shard_map/all_to_all | solution.py:133
  104.6 0.0 copy-done.4
  104.6 0.1 copy.64
  104.7 0.7 fusion.27.dd_ref
  105.4 0.3 fusion.1
  105.8 0.8 fusion.72
  106.6 9.8 %all-to-all-done.4.arr_ref = bf16[32,40,128]{2,1,0:T(8,128)(2,1)S(1)} async-done(((bf16[32,40,128]{2,1,0:T(8,128)(2,1)}), bf16[32,40,128]{2,1,0:T(8,128)(2,1)S(1)}, u32[]{:S(2)}, u32[]{:S(2)}) %all-to-all-start.4) | async-done | bytes 327712 | tf_op jit(solution)/shard_map/all_to_all | solution.py:133
  116.5 0.7 copy-done.1
  117.2 2.1 %collect_body.1 = bf16[128,128]{1,0:T(8,128)(2,1)} custom-call(bf16[32,40,128]{2,1,0:T(8,128)(2,1)} %copy-done.1, bf16[128,1024]{1,0:T(8,128)(2,1)} %get-tuple-element.17.low_ref, bf16[128,1024]{1,0:T(8,128)(2,1)} %get-tuple-element.16.high_ref, bf16[256,128]{1,0:T(8,128)(2,1)} %fusion.27.dd_ref), custom_call_target="tpu_custom_call" | custom-call | tf_op jit(solution)/shard_map/collect_body/pallas_call | solution.py:122
  119.2 4.8 %all-gather.1 = bf16[256,128]{1,0:T(8,128)(2,1)S(1)} all-gather(bf16[128,128]{1,0:T(8,128)(2,1)} %collect_body.1), channel_id=3, replica_groups=mesh['z'=8,'x'=4,'y'=8,'c'=2] {'c'}, dimensions={0}, use_global_device_ids=true | all-gather | bytes 98304 | tf_op jit(solution)/shard_map/all_gather | solution.py:147
  124.0 10.8 %all_to_all.30 = bf16[8,64,128]{2,1,0:T(8,128)(2,1)S(1)} all-to-all(bf16[8,64,128]{2,1,0:T(8,128)(2,1)S(1)} %broadcast_in_dim.88), channel_id=1, replica_groups=mesh['z'=8,'x'=4,'y'=8,'c'=2] {'y'}, dimensions={0} | all-to-all | bytes 262144 | tf_op jit(solution)/shard_map/all_to_all | solution.py:133
  134.8 3.1 %all_gather.23 = bf16[128,128]{1,0:T(8,128)(2,1)S(1)} all-gather(bf16[64,128]{1,0:T(8,128)(2,1)S(1)} %add_convert_fusion), channel_id=1, replica_groups=mesh['z'=8,'x'=4,'y'=8,'c'=2] {'c'}, dimensions={0}, use_global_device_ids=true | all-gather | bytes 49152 | tf_op jit(solution)/shard_map/all_gather | solution.py:290
  138.0 0.1 fusion.74
  138.1 0.7 copy.66
  (33 shorter events, 0.3 us)
Async XLA Ops:
  2.1 15.8 %copy-start.10 = (s32[8]{0:T(128)S(1)}, s32[8]{0:T(128)}, u32[]{:S(2)}) copy-start(s32[8]{0:T(128)} %param.27) | copy-start | bytes 100
  2.1 16.8 %copy-start.6 = (bf16[64,128]{1,0:T(8,128)(2,1)S(1)}, bf16[64,128]{1,0:T(8,128)(2,1)}, u32[]{:S(2)}) copy-start(bf16[64,128]{1,0:T(8,128)(2,1)} %param.35) | copy-start | bytes 49156
  2.1 16.8 %copy-start.7 = (bf16[64,128]{1,0:T(8,128)(2,1)S(1)}, bf16[64,128]{1,0:T(8,128)(2,1)}, u32[]{:S(2)}) copy-start(bf16[64,128]{1,0:T(8,128)(2,1)} %param.34) | copy-start | bytes 49156
  4.1 28.9 %copy-start.2 = (f32[8,1,128,256]{3,2,1,0:T(8,128)S(1)}, f32[8,1,128,256]{3,2,1,0:T(8,128)}, u32[]{:S(2)}) copy-start(f32[8,1,128,256]{3,2,1,0:T(8,128)} %param.26) | copy-start | bytes 3145732
  4.1 28.3 %all-to-all-start = ((bf16[32,8,896]{2,1,0:T(8,128)(2,1)}), bf16[32,8,896]{2,1,0:T(8,128)(2,1)S(1)}, u32[]{:S(2)}, u32[]{:S(2)}) async-start(bf16[32,8,896]{2,1,0:T(8,128)(2,1)} %project_body.1), calls=%async_computation | async-start | bytes 917504 | tf_op jit(solution)/shard_map/all_to_all | solution.py:133
  18.9 0.7 copy-start.5
  35.1 15.1 %all-to-all-start.1 = ((bf16[32,8,256]{2,1,0:T(8,128)(2,1)}), bf16[32,8,256]{2,1,0:T(8,128)(2,1)S(1)}, u32[]{:S(2)}, u32[]{:S(2)}) async-start(bf16[32,8,256]{2,1,0:T(8,128)(2,1)} %broadcast_in_dim.43), calls=%async_computation.1 | async-start | bytes 262144 | tf_op jit(solution)/shard_map/all_to_all | solution.py:133
  42.6 7.6 %copy-start.9 = (bf16[256,64]{0,1:T(8,128)(2,1)S(1)}, bf16[256,64]{0,1:T(8,128)(2,1)}, u32[]{:S(2)}) copy-start(bf16[256,64]{0,1:T(8,128)(2,1)} %param.25) | copy-start | bytes 98308
  55.6 8.2 %copy-start.3 = (bf16[256,64]{1,0:T(8,128)(2,1)S(1)}, bf16[256,64]{1,0:T(8,128)(2,1)}, u32[]{:S(2)}) copy-start(bf16[256,64]{1,0:T(8,128)(2,1)} %copy.61.res_ref) | copy-start | bytes 98308
  55.6 14.9 %all-to-all-start.2 = ((bf16[8,64,128]{2,1,0:T(8,128)(2,1)}), bf16[8,64,128]{2,1,0:T(8,128)(2,1)S(1)}, u32[]{:S(2)}, u32[]{:S(2)}) async-start(bf16[8,64,128]{2,1,0:T(8,128)(2,1)} %broadcast_in_dim.77), calls=%async_computation.2 | async-start | bytes 262144 | tf_op jit(solution)/shard_map/all_to_all | solution.py:133
  62.5 0.7 copy-start.11
  76.4 19.3 %all-to-all-start.3 = ((bf16[32,56,128]{2,1,0:T(8,128)(2,1)}), bf16[32,56,128]{2,1,0:T(8,128)(2,1)S(1)}, u32[]{:S(2)}, u32[]{:S(2)}) async-start(bf16[32,56,128]{2,1,0:T(8,128)(2,1)} %dispatch_body.1), calls=%async_computation.3 | async-start | bytes 917504 | tf_op jit(solution)/shard_map/all_to_all | solution.py:133
  80.3 0.7 copy-start.8
  95.8 0.8 copy-start
  99.5 5.1 %copy-start.4 = (bf16[128,64]{0,1:T(8,128)(2,1)S(1)}, bf16[128,64]{0,1:T(8,128)(2,1)}, u32[]{:S(2)}) copy-start(bf16[128,64]{0,1:T(8,128)(2,1)} %param.36) | copy-start | bytes 49156
  99.5 16.9 %all-to-all-start.4 = ((bf16[32,40,128]{2,1,0:T(8,128)(2,1)}), bf16[32,40,128]{2,1,0:T(8,128)(2,1)S(1)}, u32[]{:S(2)}, u32[]{:S(2)}) async-start(bf16[32,40,128]{2,1,0:T(8,128)(2,1)} %expert_body.1), calls=%async_computation.4 | async-start | bytes 655360 | tf_op jit(solution)/shard_map/all_to_all | solution.py:133
  116.5 0.7 copy-start.1

commit v2 on v1

v2 whole, which is shorter than its diff:
```python
import jax
import jax.numpy as jnp
from jax import lax
from jax.experimental import pallas as pl
from jax.experimental.pallas import tpu as pltpu
from jax.sharding import Mesh, PartitionSpec as P

D = 2048
KEY_DIM = 128
VAL_DIM = 256
EPS = 1e-06
LIMIT = 7.0
ALPHA = 1.702
F32 = jnp.float32
BF16 = jnp.bfloat16
EP = ("z", "x")


def mm(a, b):
    return jnp.dot(a, b, preferred_element_type=F32)


def dots(a, b, i, j):
    return lax.dot_general(a, b, (((i,), (j,)), ((), ())), preferred_element_type=F32)


def two_part(v):
    high = v.astype(BF16).astype(F32)
    return high, v - high


def lane_of(shape):
    return lax.broadcasted_iota(jnp.int32, shape, len(shape) - 1)


def project_body(res_ref, gain_ref, q_ref, k_ref, v_ref, g_ref, out_ref):
    rows = res_ref[...].astype(F32).T
    normed = (rows * gain_ref[...]).astype(BF16)
    at = 0
    for ref in (q_ref, k_ref, v_ref, g_ref):
        width = ref.shape[1]
        part = mm(normed, ref[...])
        out_ref[:, :, at : at + width] = part.reshape(32, 8, width).astype(BF16)
        at += width
    high, low = two_part(jnp.sum(rows * rows, axis=1, keepdims=True))
    lane = lane_of((256, 128))
    stats = jnp.where(lane == 0, high, jnp.where(lane == 1, low, 0.0))
    out_ref[:, :, at : at + 128] = stats.reshape(32, 8, 128).astype(BF16)


def retain_body(arr_ref, prior_ref, cos_ref, sin_ref, decay_ref, out_ref, key_ref, value_ref):
    summed = jnp.sum(arr_ref[...].astype(F32), axis=0)
    scale = lax.rsqrt((summed[:, 768:769] + summed[:, 769:770]) / D + EPS)
    cosine = cos_ref[...]
    sine = sin_ref[...]
    query = summed[:, 0:128] * scale
    query = query * cosine + pltpu.roll(query, 64, 1) * sine
    key = summed[:, 128:256] * scale
    key = (key * cosine + pltpu.roll(key, 64, 1) * sine) * KEY_DIM ** (-0.5)
    value = summed[:, 256:512] * scale
    gate = summed[:, 512:768] * scale
    key_ref[...] = key
    value_ref[...] = value
    turned = query.T
    reads = [
        jnp.sum(turned[:, b : b + 1] * prior_ref[b], axis=0, keepdims=True) for b in range(8)
    ]
    met = jnp.sum(query * key, axis=1, keepdims=True)
    read = decay_ref[...] * jnp.concatenate(reads, axis=0) + met * value
    normed = read * lax.rsqrt(jnp.mean(read * read, axis=1, keepdims=True) + EPS)
    gated = normed * jax.nn.silu(gate)
    out_ref[...] = jnp.broadcast_to(gated[None], (32, 8, VAL_DIM)).astype(BF16)


def dispatch_body(am_ref, sel_ref, gain_ref, dw_ref, out_ref):
    am = am_ref[...]
    none = jnp.zeros((64, 128), BF16)
    stacked = jnp.concatenate(
        [
            jnp.concatenate([am[:, :128], none], axis=1),
            jnp.concatenate([none, am[:, 128:]], axis=1),
        ],
        axis=0,
    )
    sent = dots(sel_ref[...], stacked, 1, 1)
    out_ref[:, 0:32, :] = sent.reshape(32, 32, 128).astype(BF16)
    amf = am.astype(F32)
    normed = (amf * gain_ref[:, 0:1]).astype(BF16)
    both = dots(normed, dw_ref[...], 0, 0)
    out_ref[:, 32:40, :] = both[:, :128].reshape(32, 8, 128).astype(BF16)
    out_ref[:, 40:48, :] = both[:, 128:256].reshape(32, 8, 128).astype(BF16)
    high, low = two_part(amf * amf)
    squares = jnp.concatenate([high, low], axis=0).astype(BF16)
    second = (lane_of((128, 128)) == 1).astype(F32).astype(BF16)
    stats = both[:, 256:384] + dots(squares, second, 0, 0)
    high, low = two_part(stats)
    stats = high + pltpu.roll(low, 2, 1)
    out_ref[:, 48:56, :] = stats.reshape(32, 8, 128).astype(BF16)


def expert_body(arr_ref, gain_ref, eg_ref, eu_ref, ed_ref, weight_ref, out_ref, zn_ref):
    tail = jnp.sum(arr_ref[:, 32:56, :].astype(F32), axis=0)
    stats = tail[16:24]
    scale = lax.rsqrt((stats[:, 1:2] + stats[:, 3:4]) / D + EPS)
    mix = jax.nn.sigmoid(scale * (stats[:, 0:1] + stats[:, 2:3]))
    act = jax.nn.silu(tail[0:8] * scale) * (tail[8:16] * scale) * mix
    out_ref[:, 32:40, :] = jnp.broadcast_to(act[None], (32, 8, 128)).astype(BF16)
    left = lane_of((32, 128)) < 64
    squares = jnp.zeros((64, 128), F32)
    for p in range(16):
        a = arr_ref[2 * p, 0:32, :].astype(F32)
        b = arr_ref[2 * p + 1, 0:32, :].astype(F32)
        z = jnp.concatenate(
            [
                jnp.where(left, a, pltpu.roll(b, 64, 1)),
                jnp.where(left, pltpu.roll(a, 64, 1), b),
            ],
            axis=0,
        )
        squares = squares + z * z
        zn_ref[:, 128 * p : 128 * p + 128] = (
            z * gain_ref[:, 128 * p : 128 * p + 128]
        ).astype(BF16)
    norm = lax.rsqrt(jnp.sum(squares, axis=1, keepdims=True) / D + EPS)
    zn = zn_ref[...]
    gate = jnp.minimum(mm(zn, eg_ref[...]) * norm, LIMIT)
    up = jnp.clip(mm(zn, eu_ref[...]) * norm, -LIMIT, LIMIT)
    hidden = ((up + 1.0) * gate * jax.nn.sigmoid(ALPHA * gate)).astype(BF16)
    weight = weight_ref[...]
    for p in range(16):
        o = mm(hidden, ed_ref[:, 128 * p : 128 * p + 128]) * weight
        low, high = o[0:32], o[32:64]
        out_ref[2 * p, 0:32, :] = jnp.where(left, low, pltpu.roll(high, 64, 1)).astype(BF16)
        out_ref[2 * p + 1, 0:32, :] = jnp.where(left, pltpu.roll(low, 64, 1), high).astype(BF16)


def collect_body(arr_ref, sel_ref, dd_ref, out_ref):
    slots = arr_ref[:, 0:32, :].reshape(1024, 128)
    both = dots(slots, sel_ref[...], 0, 0)
    act = arr_ref[:, 32:40, :].astype(F32).reshape(256, 128).astype(BF16)
    dense = dots(dd_ref[...], act, 1, 1)
    out_ref[:, :128] = (both[:64, :128] + dense[:, :128]).astype(BF16)
    out_ref[:, 128:] = (both[64:, 128:] + dense[:, 128:]).astype(BF16)


def call(body, out_shapes, *args, scratch=()):
    return pl.pallas_call(
        body,
        out_shape=[pltpu.VMEM(shape, kind) for shape, kind in out_shapes],
        in_specs=[pl.BlockSpec(memory_space=pltpu.VMEM)] * len(args),
        out_specs=[pl.BlockSpec(memory_space=pltpu.VMEM)] * len(out_shapes),
        scratch_shapes=list(scratch),
        name=body.__name__,
    )(*[pltpu.with_memory_space_constraint(a, pltpu.VMEM) for a in args])


def exchange(pieces, axes):
    return lax.all_to_all(pieces, axes, 0, 0, tiled=True)


def from_everyone(value, axes):
    peers = lax.axis_size(axes)
    return exchange(jnp.broadcast_to(value[None], (peers, *value.shape)), axes)


def own_half(value, core):
    rows = value.shape[0] // 2
    return lax.dynamic_slice_in_dim(value, core * rows, rows, 0)


def half_sum(partial, core):
    both = lax.all_gather(partial, "c")
    mine = lax.dynamic_slice_in_dim(both, core * 32, 32, 1).astype(F32)
    pair = (mine[0] + mine[1]).astype(BF16)
    return jnp.sum(from_everyone(pair, ("y",)).astype(F32), axis=0)


def routing(route_ids, route_weight, own):
    rows = route_ids.shape[0]
    names = jnp.arange(32, dtype=jnp.int32)
    hit = route_ids[:, :, None] == names[None, None, :]
    named = jnp.any(hit, axis=1)
    weight = jnp.sum(jnp.where(hit, route_weight[:, :, None], 0.0), axis=1)
    r = lax.broadcasted_iota(jnp.int32, (rows, rows), 0)
    q = lax.broadcasted_iota(jnp.int32, (rows, rows), 1)
    before = ((r // 8 == q // 8) & (q < r)).astype(BF16)
    earlier = mm(before, named.astype(BF16))
    group = lax.broadcasted_iota(jnp.int32, (rows, 1), 0) // 8
    place = ((group % 16) * 2).astype(F32) + earlier
    place = jnp.where(named, place, 64.0).astype(BF16)
    x = lax.broadcasted_iota(jnp.int32, (32, 1024), 0)
    slot = lax.broadcasted_iota(jnp.int32, (32, 1024), 1)
    spread = (slot // 32 == x).astype(BF16)
    tall = lax.dot_general(spread, place, (((0,), (1,)), ((), ())), preferred_element_type=F32)
    down = (lax.broadcasted_iota(jnp.int32, (1024, 1), 0) % 32).astype(F32)
    forth = (tall == down).astype(BF16)
    mine = lax.dynamic_slice_in_dim(forth, own * 32, 32, 0).astype(F32)
    own_weight = lax.dynamic_slice_in_dim(weight, own, 1, 1).reshape(1, rows)
    scaled = mine * own_weight
    slot_weight = jnp.concatenate(
        [
            jnp.sum(scaled[:, :128], axis=1, keepdims=True),
            jnp.sum(scaled[:, 128:], axis=1, keepdims=True),
        ],
        axis=0,
    )
    return forth, jnp.broadcast_to(slot_weight, (64, 128))


def per_device(
    residual,
    norm_gain,
    query_weight,
    key_weight,
    value_weight,
    gate_weight,
    out_weight,
    prior_state,
    lengths,
    ffn_gain,
    expert_gate,
    expert_up,
    expert_down,
    route_ids,
    route_weight,
    dense_gate,
    dense_up,
    dense_down,
    mix_vector,
):
    own = lax.axis_index(EP)
    core = lax.axis_index("c")
    head = lax.axis_index("y") * 2 + core
    (terms,) = call(
        project_body,
        [((32, 8, 896), BF16)],
        residual.T,
        norm_gain[None, :],
        query_weight,
        key_weight,
        value_weight,
        gate_weight,
    )
    arrived = exchange(terms, EP)

    forth, slot_weight = routing(route_ids, route_weight, own)
    gain_here = lax.dynamic_slice_in_dim(ffn_gain, own * 64, 64, 0)
    gain_here = jnp.broadcast_to(gain_here[:, None], (64, 128))
    mix_block = jnp.pad(mix_vector[:, None], ((0, 0), (0, 127)))
    dense_in = jnp.concatenate([dense_gate, dense_up, mix_block], axis=1)
    residual_half = own_half(residual.T, core).astype(F32)
    inverse = 1.0 / 10000.0 ** jnp.linspace(0.0, 1.0, 64, dtype=F32)
    angles = lengths.astype(F32)[:, None] * inverse[None, :]
    cosine = jnp.cos(angles)
    sine = jnp.sin(angles)
    cosine = jnp.concatenate([cosine, cosine], axis=1)
    sine = jnp.concatenate([-sine, sine], axis=1)
    decay = 1.0 - jnp.exp2(-1.0 - 0.5 * head.astype(F32))
    decay_row = jnp.broadcast_to(decay[None, None], (1, VAL_DIM))
    (
        arrived,
        forth,
        slot_weight,
        gain_here,
        dense_in,
        residual_half,
        cosine,
        sine,
        decay_row,
    ) = lax.optimization_barrier(
        (
            arrived,
            forth,
            slot_weight,
            gain_here,
            dense_in,
            residual_half,
            cosine,
            sine,
            decay_row,
        )
    )
    gated, key_rot, values = call(
        retain_body,
        [((32, 8, VAL_DIM), BF16), ((8, KEY_DIM), F32), ((8, VAL_DIM), F32)],
        arrived,
        prior_state[:, 0],
        cosine,
        sine,
        decay_row,
    )
    new_state = decay * prior_state + key_rot[:, None, :, None] * values[:, None, None, :]

    heads = exchange(gated, EP).reshape(256, VAL_DIM)
    attn = dots(out_weight.T, heads, 1, 1).astype(BF16)
    after_half = (residual_half + half_sum(attn, core)).astype(BF16)
    after = lax.all_gather(after_half, "c", tiled=True)

    (sent,) = call(
        dispatch_body, [((32, 56, 128), BF16)], after, forth, gain_here, dense_in
    )
    inbox = exchange(sent, EP)
    (made,) = call(
        expert_body,
        [((32, 40, 128), BF16)],
        inbox,
        ffn_gain[None, :],
        expert_gate[0],
        expert_up[0],
        expert_down[0],
        slot_weight,
        scratch=(pltpu.VMEM((64, D), BF16),),
    )
    returned = exchange(made, EP)
    (branch,) = call(collect_body, [((64, 256), BF16)], returned, forth, dense_down.T)
    out_half = (after_half.astype(F32) + half_sum(branch, core)).astype(BF16)
    layer_out = lax.all_gather(out_half, "c", tiled=True).T
    return layer_out, new_state


def solution(mesh):
    fine = Mesh(mesh.devices.reshape(8, 4, 8, 2), ("z", "x", "y", "c"))
    tp = ("y", "c")
    placed = (
        P(None, EP),
        P(EP),
        P(EP, tp),
        P(EP, tp),
        P(EP, tp),
        P(EP, tp),
        P(tp, EP),
        P(EP, tp, None, None),
        P(EP),
        P(),
        P(EP, None, tp),
        P(EP, None, tp),
        P(EP, tp, None),
        P(),
        P(),
        P(EP, tp),
        P(EP, tp),
        P(tp, EP),
        P(EP),
    )
    return jax.shard_map(
        per_device,
        mesh=fine,
        in_specs=placed,
        out_specs=(P(None, EP), P(EP, tp, None, None)),
        check_vma=False,
    )
```

time: 140 us -> 134 us (0.957)
  blocking collectives: 26.9 us -> 80.6 us
  waiting for transfers between devices: 50.4 us -> 18.6 us
  starting transfers between devices: 35.5 us -> 17.2 us
  Pallas kernels: 9.1 us -> 3.27 us
  other arithmetic: 5.81 us -> 1.84 us
    all_to_all x1 -> x4, blocking collectives: 10.8 us -> 63.8 us  [exchange(): return lax.all_to_all(pieces, axes, 0, 0, tiled=True)]
    all_to_all x5 -> x2, waiting for transfers between devices: 50.4 us -> 18.6 us  [exchange(): return lax.all_to_all(pieces, axes, 0, 0, tiled=True)]
    all_to_all x5 -> x2, starting transfers between devices: 35.5 us -> 17.2 us  [exchange(): return lax.all_to_all(pieces, axes, 0, 0, tiled=True)]
    pallas_call x4 -> x5, Pallas kernels: 9.1 us -> 3.27 us  [call(): pl.pallas_call(body, out_shape=[pltpu.VMEM(shape, kind) for shape, kind i...]
    unnamed x27 -> x43, local copies, waits for them, and re-layouts: 4.45 us -> 8.53 us
    reduce_sum x3 -> x0, other arithmetic: 1.49 us -> none  [the longest x1 1.3 us: per_device(): read = jnp.sum(query_rot[:, :, None] * new_state[:, 0], axis=1)]
  transfers between devices with their start and end apart: 5 -> 2, of which waited for: 5 -> 2; matrix products, arithmetic and copies ran while one was open for 5% -> 2% of each run, Pallas kernels for 0% -> 0%
where the time goes in v2:
time: 134 us; the launch traced here: 133 us
  blocking collectives  80.6 us (60%)
  waiting for transfers between devices  18.6 us (14%)
  starting transfers between devices  17.2 us (13%)
  local copies, waits for them, and re-layouts  9.54 us (7%)
  Pallas kernels  3.27 us (2%)
  other arithmetic  1.84 us (1%)
    all_to_all x4, blocking collectives, exchange(): return lax.all_to_all(pieces, axes, 0, 0, tiled=True)  63.8 us
    all_to_all x2, waiting for transfers between devices, exchange(): return lax.all_to_all(pieces, axes, 0, 0, tiled=True)  18.6 us
    all_to_all x2, starting transfers between devices, exchange(): return lax.all_to_all(pieces, axes, 0, 0, tiled=True)  17.2 us
    all_gather x2, blocking collectives, half_sum(): both = lax.all_gather(partial, 'c')  10.1 us
    unnamed x43, local copies, waits for them, and re-layouts  8.53 us
    all_gather x1, blocking collectives, per_device(): after = lax.all_gather(after_half, 'c', tiled=True)  3.56 us
    pallas_call x5, Pallas kernels, call(): pl.pallas_call(body, out_shape=[pltpu.VMEM(shape, kind) for shape, kind i...  3.27 us
    all_gather x1, blocking collectives, per_device(): layer_out = lax.all_gather(out_half, 'c', tiled=True).T  3.12 us
  transfers between devices with their start and end apart: 2, of which 2 were waited for; matrix products, arithmetic and copies ran while one was open for 2% of the time, Pallas kernels for 0%

profile of v2, /device:TPU:1, one launch (start us, length us, event | category | flops | bytes accessed | tf_op | source)
XLA Modules:
  0.0 132.8 jit_solution(2803643666118540452)
XLA Ops:
  0.6 0.0 copy-start
  0.6 0.0 copy-start.14
  0.7 0.7 copy-done.14
  1.3 0.0 copy-start.7
  1.3 0.8 copy-done.7
  2.1 0.0 copy-start.8
  2.1 0.8 copy-done.8
  2.8 0.0 copy-start.9
  2.8 0.8 copy-done.9
  3.6 0.0 copy-start.11
  3.6 0.7 copy-done.11
  4.3 0.0 copy-start.12
  4.3 0.7 copy-done.12
  5.0 1.1 project_body.1
  6.1 13.8 %all-to-all-start = ((bf16[32,8,896]{2,1,0:T(8,128)(2,1)}), bf16[32,8,896]{2,1,0:T(8,128)(2,1)S(1)}, u32[]{:S(2)}, u32[]{:S(2)}) async-start(bf16[32,8,896]{2,1,0:T(8,128)(2,1)} %project_body.1), calls=%async_computation | async-start | bytes 917504 | tf_op jit(solution)/shard_map/all_to_all | solution.py:158
  20.1 0.0 copy-done.20
  20.1 0.0 copy-done.15
  20.2 0.0 copy-done.19
  20.2 0.1 copy.27
  20.3 0.0 copy-done.18
  20.3 0.0 copy-start.13
  20.3 0.7 copy-done.13
  21.0 0.1 dynamic_slice.20
  21.1 0.6 fusion.sel_ref
  21.7 0.0 copy-start.2
  21.8 0.1 fusion.45
  21.9 0.1 slice_reduce_fusion.1
  22.0 0.1 maximum_bitcast_fusion
  22.0 0.1 fusion.43
  22.2 0.1 pad_maximum_fusion
  22.3 0.7 copy-done.16
  23.0 0.0 copy-done.17
  23.0 11.4 %all-to-all-done.arr_ref = bf16[32,8,896]{2,1,0:T(8,128)(2,1)S(1)} async-done(((bf16[32,8,896]{2,1,0:T(8,128)(2,1)}), bf16[32,8,896]{2,1,0:T(8,128)(2,1)S(1)}, u32[]{:S(2)}, u32[]{:S(2)}) %all-to-all-start) | async-done | bytes 458784 | tf_op jit(solution)/shard_map/all_to_all | solution.py:158
  34.4 0.1 broadcast_in_dim.83.gain_ref
  34.5 0.1 broadcast_in_dim.82.weight_ref
  34.6 0.0 copy-done.1
  34.6 0.7 retain_body.1
  35.3 14.9 %all_to_all.30 = bf16[32,8,256]{2,1,0:T(8,128)(2,1)S(1)} all-to-all(bf16[32,8,256]{2,1,0:T(8,128)(2,1)S(1)} %get-tuple-element.19), channel_id=1, replica_groups=mesh['z'=8,'x'=4,'y'=8,'c'=2] {'z','x'}, dimensions={0} | all-to-all | bytes 262144 | tf_op jit(solution)/shard_map/all_to_all | solution.py:158
  50.2 0.0 copy-done
  50.2 0.2 fusion.1
  50.3 4.6 %all-gather = bf16[128,256]{1,0:T(8,128)(2,1)S(1)} all-gather(bf16[64,256]{1,0:T(8,128)(2,1)S(1)} %fusion.1), channel_id=2, replica_groups=mesh['z'=8,'x'=4,'y'=8,'c'=2] {'c'}, dimensions={0}, use_global_device_ids=true | all-gather | bytes 98304 | tf_op jit(solution)/shard_map/all_gather | solution.py:172
  54.9 14.6 %all_to_all.31 = bf16[8,32,256]{2,1,0:T(8,128)(2,1)S(1)} all-to-all(bf16[8,32,256]{2,1,0:T(8,128)(2,1)S(1)} %broadcast_in_dim.87), channel_id=1, replica_groups=mesh['z'=8,'x'=4,'y'=8,'c'=2] {'y'}, dimensions={0} | all-to-all | bytes 262144 | tf_op jit(solution)/shard_map/all_to_all | solution.py:158
  69.5 3.6 %all_gather.20.am_ref = bf16[64,256]{1,0:T(8,128)(2,1)S(1)} all-gather(bf16[32,256]{1,0:T(8,128)(2,1)S(1)} %add_convert_fusion.1), channel_id=1, replica_groups=mesh['z'=8,'x'=4,'y'=8,'c'=2] {'c'}, dimensions={0}, use_global_device_ids=true | all-gather | bytes 49152 | tf_op jit(solution)/shard_map/all_gather | solution.py:297
  73.1 0.0 copy-done.2
  73.1 0.5 dispatch_body.1
  73.5 0.0 copy-start.6
  73.6 18.6 %all_to_all.32.arr_ref = bf16[32,56,128]{2,1,0:T(8,128)(2,1)S(1)} all-to-all(bf16[32,56,128]{2,1,0:T(8,128)(2,1)S(1)} %dispatch_body.1), channel_id=1, replica_groups=mesh['z'=8,'x'=4,'y'=8,'c'=2] {'z','x'}, dimensions={0} | all-to-all | bytes 917504 | tf_op jit(solution)/shard_map/all_to_all | solution.py:158
  92.1 0.0 copy-done.6
  92.1 1.0 copy-done.4
  93.2 1.0 copy-done.5
  94.2 0.7 expert_body.1
  95.0 0.0 copy-start.3
  95.0 0.0 copy-start.10
  95.0 15.8 %all_to_all.33.arr_ref = bf16[32,40,128]{2,1,0:T(8,128)(2,1)S(1)} all-to-all(bf16[32,40,128]{2,1,0:T(8,128)(2,1)S(1)} %expert_body.1), channel_id=1, replica_groups=mesh['z'=8,'x'=4,'y'=8,'c'=2] {'z','x'}, dimensions={0} | all-to-all | bytes 655360 | tf_op jit(solution)/shard_map/all_to_all | solution.py:158
  110.8 0.0 copy-done.3
  110.8 0.0 copy-done.10
  110.8 0.3 collect_body.1
  111.1 5.5 %all-gather.1 = bf16[128,256]{1,0:T(8,128)(2,1)S(1)} all-gather(bf16[64,256]{1,0:T(8,128)(2,1)S(1)} %collect_body.1), channel_id=3, replica_groups=mesh['z'=8,'x'=4,'y'=8,'c'=2] {'c'}, dimensions={0}, use_global_device_ids=true | all-gather | bytes 98304 | tf_op jit(solution)/shard_map/all_gather | solution.py:172
  116.7 0.7 broadcast_in_dim.90
  117.3 3.4 %all-to-all-start.5 = ((bf16[8,32,256]{2,1,0:T(8,128)(2,1)}), bf16[8,32,256]{2,1,0:T(8,128)(2,1)S(1)}, u32[]{:S(2)}, u32[]{:S(2)}) async-start(bf16[8,32,256]{2,1,0:T(8,128)(2,1)} %broadcast_in_dim.90), calls=%async_computation.5 | async-start | bytes 262144 | tf_op jit(solution)/shard_map/all_to_all | solution.py:158
  120.7 1.2 multiply_add_fusion
  121.9 7.1 %all-to-all-done.5 = bf16[8,32,256]{2,1,0:T(8,128)(2,1)S(1)} async-done(((bf16[8,32,256]{2,1,0:T(8,128)(2,1)}), bf16[8,32,256]{2,1,0:T(8,128)(2,1)S(1)}, u32[]{:S(2)}, u32[]{:S(2)}) %all-to-all-start.5) | async-done | bytes 131104 | tf_op jit(solution)/shard_map/all_to_all | solution.py:158
  129.0 3.1 %all_gather.23 = bf16[64,256]{1,0:T(8,128)(2,1)S(1)} all-gather(bf16[32,256]{1,0:T(8,128)(2,1)S(1)} %add_convert_fusion), channel_id=1, replica_groups=mesh['z'=8,'x'=4,'y'=8,'c'=2] {'c'}, dimensions={0}, use_global_device_ids=true | all-gather | bytes 49152 | tf_op jit(solution)/shard_map/all_gather | solution.py:317
  132.1 0.6 copy.29
  (33 shorter events, 0.2 us)
Async XLA Ops:
  0.6 49.5 %copy-start = (bf16[256,64]{0,1:T(8,128)(2,1)S(1)}, bf16[256,64]{0,1:T(8,128)(2,1)}, u32[]{:S(2)}) copy-start(bf16[256,64]{0,1:T(8,128)(2,1)} %param.25) | copy-start | bytes 98308
  0.6 0.7 copy-start.14
  1.3 0.8 copy-start.7
  2.1 0.8 copy-start.8
  2.8 0.8 copy-start.9
  3.6 0.7 copy-start.11
  4.3 0.7 copy-start.12
  5.0 15.1 %copy-start.20 = (s32[8]{0:T(128)S(1)}, s32[8]{0:T(128)}, u32[]{:S(2)}) copy-start(s32[8]{0:T(128)} %param.27) | copy-start | bytes 100
  5.0 15.1 %copy-start.15 = (s32[256,4]{0,1:T(4,128)S(1)}, s32[256,4]{0,1:T(4,128)}, u32[]{:S(2)}) copy-start(s32[256,4]{0,1:T(4,128)} %param.32) | copy-start | bytes 12292
  5.0 15.2 %copy-start.19 = (bf16[64]{0:T(256)(128)(2,1)S(1)}, bf16[64]{0:T(256)(128)(2,1)}, u32[]{:S(2)}) copy-start(bf16[64]{0:T(256)(128)(2,1)} %param.37) | copy-start | bytes 388
  5.0 15.3 %copy-start.18 = (f32[256,4]{0,1:T(4,128)S(1)}, f32[256,4]{0,1:T(4,128)}, u32[]{:S(2)}) copy-start(f32[256,4]{0,1:T(4,128)} %param.33) | copy-start | bytes 12292
  6.1 28.4 %copy-start.1 = (f32[8,1,128,256]{3,2,1,0:T(8,128)S(1)}, f32[8,1,128,256]{3,2,1,0:T(8,128)}, u32[]{:S(2)}) copy-start(f32[8,1,128,256]{3,2,1,0:T(8,128)} %param.26) | copy-start | bytes 3145732
  6.1 28.3 %all-to-all-start = ((bf16[32,8,896]{2,1,0:T(8,128)(2,1)}), bf16[32,8,896]{2,1,0:T(8,128)(2,1)S(1)}, u32[]{:S(2)}, u32[]{:S(2)}) async-start(bf16[32,8,896]{2,1,0:T(8,128)(2,1)} %project_body.1), calls=%async_computation | async-start | bytes 917504 | tf_op jit(solution)/shard_map/all_to_all | solution.py:158
  20.3 0.7 copy-start.13
  21.7 51.3 %copy-start.2 = (bf16[1024,256]{1,0:T(8,128)(2,1)}, bf16[1024,256]{1,0:T(8,128)(2,1)S(1)}, u32[]{:S(2)}) copy-start(bf16[1024,256]{1,0:T(8,128)(2,1)S(1)} %fusion.sel_ref) | copy-start | bytes 1572868
  22.2 0.7 copy-start.16
  22.2 0.7 copy-start.17
  73.5 18.6 %copy-start.6 = (bf16[1,128,2048]{2,1,0:T(8,128)(2,1)S(1)}, bf16[1,128,2048]{2,1,0:T(8,128)(2,1)}, u32[]{:S(2)}) copy-start(bf16[1,128,2048]{2,1,0:T(8,128)(2,1)} %param.31) | copy-start | bytes 1572868
  92.1 1.0 copy-start.4
  93.2 1.0 copy-start.5
  95.0 15.9 %copy-start.3 = (bf16[1024,256]{1,0:T(8,128)(2,1)S(1)}, bf16[1024,256]{1,0:T(8,128)(2,1)}, u32[]{:S(2)}) copy-start(bf16[1024,256]{1,0:T(8,128)(2,1)} %copy-done.2) | copy-start | bytes 1572868
  95.0 15.8 %copy-start.10 = (bf16[128,64]{0,1:T(8,128)(2,1)S(1)}, bf16[128,64]{0,1:T(8,128)(2,1)}, u32[]{:S(2)}) copy-start(bf16[128,64]{0,1:T(8,128)(2,1)} %param.36) | copy-start | bytes 49156
  117.3 11.7 %all-to-all-start.5 = ((bf16[8,32,256]{2,1,0:T(8,128)(2,1)}), bf16[8,32,256]{2,1,0:T(8,128)(2,1)S(1)}, u32[]{:S(2)}, u32[]{:S(2)}) async-start(bf16[8,32,256]{2,1,0:T(8,128)(2,1)} %broadcast_in_dim.90), calls=%async_computation.5 | async-start | bytes 262144 | tf_op jit(solution)/shard_map/all_to_all | solution.py:158

commit v3 on v2

v3 whole, which is shorter than its diff:
```python
import jax
import jax.numpy as jnp
from jax import lax
from jax.experimental import pallas as pl
from jax.experimental.pallas import tpu as pltpu
from jax.sharding import Mesh, PartitionSpec as P

D = 2048
KEY_DIM = 128
VAL_DIM = 256
EPS = 1e-06
LIMIT = 7.0
ALPHA = 1.702
F32 = jnp.float32
BF16 = jnp.bfloat16
EP = ("z", "x")


def mm(a, b):
    return jnp.dot(a, b, preferred_element_type=F32)


def dots(a, b, i, j):
    return lax.dot_general(a, b, (((i,), (j,)), ((), ())), preferred_element_type=F32)


def two_part(v):
    high = v.astype(BF16).astype(F32)
    return high, v - high


def lane_of(shape):
    return lax.broadcasted_iota(jnp.int32, shape, len(shape) - 1)


def project_body(res_ref, gain_ref, q_ref, k_ref, v_ref, g_ref, out_ref):
    rows = res_ref[...].astype(F32).T
    normed = (rows * gain_ref[...]).astype(BF16)
    at = 0
    for ref in (q_ref, k_ref, v_ref, g_ref):
        width = ref.shape[1]
        part = mm(normed, ref[...])
        out_ref[:, :, at : at + width] = part.reshape(32, 8, width).astype(BF16)
        at += width
    high, low = two_part(jnp.sum(rows * rows, axis=1, keepdims=True))
    lane = lane_of((256, 128))
    stats = jnp.where(lane == 0, high, jnp.where(lane == 1, low, 0.0))
    out_ref[:, :, at : at + 128] = stats.reshape(32, 8, 128).astype(BF16)


def retain_body(arr_ref, prior_ref, cos_ref, sin_ref, decay_ref, out_ref, key_ref, value_ref):
    summed = jnp.sum(arr_ref[...].astype(F32), axis=0)
    scale = lax.rsqrt((summed[:, 768:769] + summed[:, 769:770]) / D + EPS)
    cosine = cos_ref[...]
    sine = sin_ref[...]
    query = summed[:, 0:128] * scale
    query = query * cosine + pltpu.roll(query, 64, 1) * sine
    key = summed[:, 128:256] * scale
    key = (key * cosine + pltpu.roll(key, 64, 1) * sine) * KEY_DIM ** (-0.5)
    value = summed[:, 256:512] * scale
    gate = summed[:, 512:768] * scale
    key_ref[...] = key
    value_ref[...] = value
    turned = query.T
    reads = [
        jnp.sum(turned[:, b : b + 1] * prior_ref[b], axis=0, keepdims=True) for b in range(8)
    ]
    met = jnp.sum(query * key, axis=1, keepdims=True)
    read = decay_ref[...] * jnp.concatenate(reads, axis=0) + met * value
    normed = read * lax.rsqrt(jnp.mean(read * read, axis=1, keepdims=True) + EPS)
    gated = normed * jax.nn.silu(gate)
    out_ref[...] = jnp.broadcast_to(gated[None], (32, 8, VAL_DIM)).astype(BF16)


def dispatch_body(am_ref, sel_ref, gain_ref, dense_ref, mix_ref, out_ref):
    am = am_ref[...].astype(F32)
    left = lane_of((64, 128)) < 64
    stacked = jnp.concatenate([jnp.where(left, am, 0.0), jnp.where(left, 0.0, am)], axis=0)
    sent = dots(sel_ref[...], stacked.astype(BF16), 1, 1)
    out_ref[:, 0:16, :] = sent.reshape(32, 16, 128).astype(BF16)
    normed = (am * gain_ref[:, 0:1]).astype(BF16)
    high, low = two_part(am * am)
    squares = jnp.concatenate([high, low], axis=0).astype(BF16)
    second = (lane_of((128, 128)) == 1).astype(F32).astype(BF16)
    stats = dots(normed, mix_ref[...], 0, 0) + dots(squares, second, 0, 0)
    high, low = two_part(stats)
    stats = (high + pltpu.roll(low, 2, 1)).reshape(16, 8, 128).astype(BF16)
    for half in range(2):
        at = 16 * half
        both = dots(normed, dense_ref[half, :, 0:256], 0, 0)
        out_ref[at : at + 16, 16:24, :] = both[:, :128].reshape(16, 8, 128).astype(BF16)
        out_ref[at : at + 16, 24:32, :] = both[:, 128:].reshape(16, 8, 128).astype(BF16)
        out_ref[at : at + 16, 32:40, :] = stats


def expert_body(
    arr_ref,
    gain_ref,
    eg_ref,
    eu_ref,
    pg_ref,
    pu_ref,
    weight_ref,
    ed_ref,
    pd_ref,
    out_ref,
    zn_ref,
    own_down,
    other_down,
    sems,
):
    first = pltpu.make_async_copy(ed_ref, own_down, sems.at[0])
    second = pltpu.make_async_copy(pd_ref, other_down, sems.at[1])
    first.start()
    second.start()
    tail = jnp.sum(arr_ref[:, 16:40, :].astype(F32), axis=0)
    stats = tail[16:24]
    scale = lax.rsqrt((stats[:, 1:2] + stats[:, 3:4]) / D + EPS)
    mix = jax.nn.sigmoid(scale * (stats[:, 0:1] + stats[:, 2:3]))
    act = jax.nn.silu(tail[0:8] * scale) * (tail[8:16] * scale) * mix
    out_ref[:, 16:24, :] = jnp.broadcast_to(act[None], (32, 8, 128)).astype(BF16)
    left = lane_of((16, 128)) < 64
    squares = jnp.zeros((32, 128), F32)
    for p in range(16):
        a = arr_ref[2 * p, 0:16, :].astype(F32)
        b = arr_ref[2 * p + 1, 0:16, :].astype(F32)
        z = jnp.concatenate(
            [
                jnp.where(left, a, pltpu.roll(b, 64, 1)),
                jnp.where(left, pltpu.roll(a, 64, 1), b),
            ],
            axis=0,
        )
        squares = squares + z * z
        zn_ref[:, 128 * p : 128 * p + 128] = (
            z * gain_ref[:, 128 * p : 128 * p + 128]
        ).astype(BF16)
    norm = lax.rsqrt(jnp.sum(squares, axis=1, keepdims=True) / D + EPS)
    zn = zn_ref[...]

    def hidden_of(gate_w, up_w):
        gate = jnp.minimum(mm(zn, gate_w[...]) * norm, LIMIT)
        up = jnp.clip(mm(zn, up_w[...]) * norm, -LIMIT, LIMIT)
        return ((up + 1.0) * gate * jax.nn.sigmoid(ALPHA * gate)).astype(BF16)

    own = hidden_of(eg_ref, eu_ref)
    other = hidden_of(pg_ref, pu_ref)
    weight = weight_ref[...]
    first.wait()
    second.wait()
    for p in range(16):
        at = slice(128 * p, 128 * p + 128)
        o = (mm(own, own_down[:, at]) + mm(other, other_down[:, at])) * weight
        low, high = o[0:16], o[16:32]
        out_ref[2 * p, 0:16, :] = jnp.where(left, low, pltpu.roll(high, 64, 1)).astype(BF16)
        out_ref[2 * p + 1, 0:16, :] = jnp.where(left, pltpu.roll(low, 64, 1), high).astype(BF16)


def collect_body(arr_ref, sel_ref, dense_ref, out_ref):
    slots = arr_ref[:, 0:16, :].reshape(512, 128)
    both = dots(slots, sel_ref[...], 0, 0)
    routed = jnp.where(lane_of((64, 128)) < 64, both[:64], both[64:])
    act = arr_ref[:, 16:24, :].astype(F32).reshape(256, 128).astype(BF16)
    dense = dots(dense_ref[0, :, 256:384], act[:128], 1, 1)
    dense = dense + dots(dense_ref[1, :, 256:384], act[128:], 1, 1)
    out_ref[...] = (routed + dense).astype(BF16)


def call(body, out_shapes, *args, far=(), scratch=(), near=True):
    if near:
        args = [pltpu.with_memory_space_constraint(a, pltpu.VMEM) for a in args]
    inside = pl.BlockSpec(memory_space=pltpu.VMEM)
    outside = pl.BlockSpec(memory_space=pl.ANY)
    return pl.pallas_call(
        body,
        out_shape=[pltpu.VMEM(shape, kind) for shape, kind in out_shapes],
        in_specs=[inside] * len(args) + [outside] * len(far),
        out_specs=[inside] * len(out_shapes),
        scratch_shapes=list(scratch),
        name=body.__name__,
    )(*args, *far)


def exchange(pieces, axes):
    return lax.all_to_all(pieces, axes, 0, 0, tiled=True)


def from_everyone(value, axes):
    peers = lax.axis_size(axes)
    return exchange(jnp.broadcast_to(value[None], (peers, *value.shape)), axes)


def own_half(value, core, dim):
    size = value.shape[dim] // 2
    return lax.dynamic_slice_in_dim(value, core * size, size, dim)


def sum_over_y(partial):
    return jnp.sum(from_everyone(partial, ("y",)).astype(F32), axis=0)


def partner(value):
    return lax.ppermute(value, "c", [(0, 1), (1, 0)])


def routing(route_ids, route_weight, own, core):
    rows = route_ids.shape[0]
    names = jnp.arange(32, dtype=jnp.int32)
    hit = route_ids[:, :, None] == names[None, None, :]
    named = jnp.any(hit, axis=1)
    weight = jnp.sum(jnp.where(hit, route_weight[:, :, None], 0.0), axis=1)
    r = lax.broadcasted_iota(jnp.int32, (rows, rows), 0)
    q = lax.broadcasted_iota(jnp.int32, (rows, rows), 1)
    before = ((r // 8 == q // 8) & (q < r)).astype(BF16)
    earlier = mm(before, named.astype(BF16))
    group = lax.broadcasted_iota(jnp.int32, (rows, 1), 0) // 8
    place = ((group % 8) * 2).astype(F32) + earlier
    place = own_half(jnp.where(named, place, 64.0).astype(BF16), core, 0)
    x = lax.broadcasted_iota(jnp.int32, (32, 512), 0)
    slot = lax.broadcasted_iota(jnp.int32, (32, 512), 1)
    spread = (slot // 16 == x).astype(BF16)
    tall = dots(spread, place, 0, 1)
    down = (lax.broadcasted_iota(jnp.int32, (512, 1), 0) % 16).astype(F32)
    select = (tall == down).astype(BF16)
    mine = lax.dynamic_slice_in_dim(select, own * 16, 16, 0).astype(F32)
    own_weight = lax.dynamic_slice_in_dim(own_half(weight, core, 0), own, 1, 1).reshape(1, 128)
    scaled = mine * own_weight
    slot_weight = jnp.concatenate(
        [
            jnp.sum(scaled[:, :64], axis=1, keepdims=True),
            jnp.sum(scaled[:, 64:], axis=1, keepdims=True),
        ],
        axis=0,
    )
    return select, jnp.broadcast_to(slot_weight, (32, 128))


def per_device(
    residual,
    norm_gain,
    query_weight,
    key_weight,
    value_weight,
    gate_weight,
    out_weight,
    prior_state,
    lengths,
    ffn_gain,
    expert_gate,
    expert_up,
    expert_down,
    route_ids,
    route_weight,
    dense_gate,
    dense_up,
    dense_down,
    mix_vector,
):
    own = lax.axis_index(EP)
    core = lax.axis_index("c")
    head = lax.axis_index("y") * 2 + core
    (terms,) = call(
        project_body,
        [((32, 8, 896), BF16)],
        residual.T,
        norm_gain[None, :],
        query_weight,
        key_weight,
        value_weight,
        gate_weight,
        near=False,
    )
    arrived = exchange(terms, EP)

    select, slot_weight = routing(route_ids, route_weight, own, core)
    gain_here = lax.dynamic_slice_in_dim(ffn_gain, own * 64, 64, 0)
    gain_here = jnp.broadcast_to(gain_here[:, None], (64, 128))
    mix_block = jnp.pad(mix_vector[:, None], ((0, 0), (0, 127)))
    dense = jnp.concatenate([dense_gate, dense_up, dense_down.T], axis=1)
    dense = lax.all_gather(dense, "c")
    other_gate = partner(expert_gate[0])
    residual_half = own_half(residual.T, core, 1).astype(F32)
    inverse = 1.0 / 10000.0 ** jnp.linspace(0.0, 1.0, 64, dtype=F32)
    angles = lengths.astype(F32)[:, None] * inverse[None, :]
    cosine = jnp.cos(angles)
    sine = jnp.sin(angles)
    cosine = jnp.concatenate([cosine, cosine], axis=1)
    sine = jnp.concatenate([-sine, sine], axis=1)
    decay = 1.0 - jnp.exp2(-1.0 - 0.5 * head.astype(F32))
    decay_row = jnp.broadcast_to(decay[None, None], (1, VAL_DIM))
    (
        arrived,
        select,
        slot_weight,
        gain_here,
        mix_block,
        dense,
        other_gate,
        residual_half,
        cosine,
        sine,
        decay_row,
    ) = lax.optimization_barrier(
        (
            arrived,
            select,
            slot_weight,
            gain_here,
            mix_block,
            dense,
            other_gate,
            residual_half,
            cosine,
            sine,
            decay_row,
        )
    )
    gated, key_rot, values = call(
        retain_body,
        [((32, 8, VAL_DIM), BF16), ((8, KEY_DIM), F32), ((8, VAL_DIM), F32)],
        arrived,
        prior_state[:, 0],
        cosine,
        sine,
        decay_row,
    )
    heads = exchange(gated, EP).reshape(256, VAL_DIM)

    new_state = decay * prior_state + key_rot[:, None, :, None] * values[:, None, None, :]
    other_up, other_down, _ = lax.optimization_barrier((expert_up[0], expert_down[0], cosine))
    other_up = partner(other_up)
    other_down = partner(other_down)
    heads, new_state, other_up, other_down = lax.optimization_barrier(
        (heads, new_state, other_up, other_down)
    )

    attn = dots(out_weight.T, heads, 1, 1).astype(BF16)
    pair = own_half(lax.all_gather(attn, "c"), core, 2).astype(F32)
    after_half = (residual_half + sum_over_y((pair[0] + pair[1]).astype(BF16))).astype(BF16)
    (sent,) = call(
        dispatch_body,
        [((32, 40, 128), BF16)],
        after_half,
        select,
        gain_here,
        dense,
        mix_block,
    )
    inbox = exchange(sent, EP)
    (made,) = call(
        expert_body,
        [((32, 24, 128), BF16)],
        inbox,
        ffn_gain[None, :],
        expert_gate[0],
        expert_up[0],
        other_gate,
        other_up,
        slot_weight,
        far=(expert_down[0], other_down),
        scratch=(
            pltpu.VMEM((32, D), BF16),
            pltpu.VMEM((128, D), BF16),
            pltpu.VMEM((128, D), BF16),
            pltpu.SemaphoreType.DMA((2,)),
        ),
    )
    returned = exchange(made, EP)
    (branch,) = call(collect_body, [((64, 128), BF16)], returned, select, dense)
    out_half = (after_half.astype(F32) + sum_over_y(branch)).astype(BF16)
    layer_out = lax.all_gather(out_half, "c")
    layer_out = jnp.transpose(layer_out, (0, 2, 1)).reshape(256, 64)
    return layer_out, new_state


def solution(mesh):
    fine = Mesh(mesh.devices.reshape(8, 4, 8, 2), ("z", "x", "y", "c"))
    tp = ("y", "c")
    placed = (
        P(None, EP),
        P(EP),
        P(EP, tp),
        P(EP, tp),
        P(EP, tp),
        P(EP, tp),
        P(tp, EP),
        P(EP, tp, None, None),
        P(EP),
        P(),
        P(EP, None, tp),
        P(EP, None, tp),
        P(EP, tp, None),
        P(),
        P(),
        P(EP, tp),
        P(EP, tp),
        P(tp, EP),
        P(EP),
    )
    return jax.shard_map(
        per_device,
        mesh=fine,
        in_specs=placed,
        out_specs=(P(None, EP), P(EP, tp, None, None)),
        check_vma=False,
    )
```

time: 134 us -> 123 us (0.918)
  blocking collectives: 80.6 us -> 66.5 us
  starting transfers between devices: 17.2 us -> 27.7 us
  local copies, waits for them, and re-layouts: 9.54 us -> 2.18 us
  waiting for transfers between devices: 18.6 us -> 15 us
  Pallas kernels: 3.27 us -> 6.76 us
    ppermute x0 -> x3, starting transfers between devices: none -> 9.71 us  [partner(): return lax.ppermute(value, 'c', [(0, 1), (1, 0)])]
    all_to_all x4, blocking collectives: 63.8 us -> 54.7 us  [exchange(): return lax.all_to_all(pieces, axes, 0, 0, tiled=True)]
    unnamed x43 -> x28, local copies, waits for them, and re-layouts: 8.53 us -> 1.03 us
    all_gather x4 -> x3, blocking collectives: 16.8 us -> 11.8 us  [the longest x1 6.16 us: per_device(): layer_out = lax.all_gather(out_half, 'c')]
    all_to_all x2, waiting for transfers between devices: 18.6 us -> 15 us  [exchange(): return lax.all_to_all(pieces, axes, 0, 0, tiled=True)]
    pallas_call x5, Pallas kernels: 3.27 us -> 6.76 us  [call(): pl.pallas_call(body, out_shape=[pltpu.VMEM(shape, kind) for shape, kind i...]
  transfers between devices with their start and end apart: 2 -> 5, of which waited for: 2 -> 2; matrix products, arithmetic and copies ran while one was open for 2% -> 2% of each run, Pallas kernels for 0% -> 1%
where the time goes in v3:
time: 123 us; the launch traced here: 122 us
  blocking collectives  66.5 us (54%)
  starting transfers between devices  27.7 us (23%)
  waiting for transfers between devices  15 us (12%)
  Pallas kernels  6.76 us (5%)
  local copies, waits for them, and re-layouts  2.18 us (2%)
  other arithmetic  1.89 us (2%)
    all_to_all x4, blocking collectives, exchange(): return lax.all_to_all(pieces, axes, 0, 0, tiled=True)  54.7 us
    all_to_all x2, starting transfers between devices, exchange(): return lax.all_to_all(pieces, axes, 0, 0, tiled=True)  18 us
    all_to_all x2, waiting for transfers between devices, exchange(): return lax.all_to_all(pieces, axes, 0, 0, tiled=True)  15 us
    ppermute x3, starting transfers between devices, partner(): return lax.ppermute(value, 'c', [(0, 1), (1, 0)])  9.71 us
    pallas_call x5, Pallas kernels, call(): pl.pallas_call(body, out_shape=[pltpu.VMEM(shape, kind) for shape, kind i...  6.76 us
    all_gather x1, blocking collectives, per_device(): layer_out = lax.all_gather(out_half, 'c')  6.16 us
    all_gather x1, blocking collectives, per_device(): pair = own_half(lax.all_gather(attn, 'c'), core, 2).astype(F32)  3.62 us
  transfers between devices with their start and end apart: 5, of which 2 were waited for; matrix products, arithmetic and copies ran while one was open for 2% of the time, Pallas kernels for 1%

profile of v3, /device:TPU:1, one launch (start us, length us, event | category | flops | bytes accessed | tf_op | source)
XLA Modules:
  0.0 121.8 jit_solution(4177156996694521303)
XLA Ops:
  0.6 0.0 copy-start
  0.7 0.0 copy-start.2
  0.7 0.0 copy-start.13
  0.7 0.0 copy-start.7
  0.7 0.0 copy-start.12
  0.7 0.0 copy-start.11
  0.7 0.0 copy-start.9
  0.7 0.0 copy-start.10
  0.7 1.9 %project_body.1 = bf16[32,8,896]{2,1,0:T(8,128)(2,1)} custom-call(bf16[64,256]{1,0:T(8,128)(2,1)} %bitcast.45, f32[1,64]{1,0:T(1,128)} %bitcast.51, bf16[64,128]{1,0:T(8,128)(2,1)} %q_ref.1, bf16[64,128]{1,0:T(8,128)(2,1)} %k_ref.1, bf16[64,256]{1,0:T(8,128)(2,1)} %v_ref.1, bf16[64,256]{1,0:T(8,128)(2,1)} %g_ref.1), custom_call_target="tpu_custom_call" | custom-call | tf_op jit(solution)/shard_map/project_body/pallas_call | solution.py:174
  2.7 13.8 %all-to-all-start = ((bf16[32,8,896]{2,1,0:T(8,128)(2,1)}), bf16[32,8,896]{2,1,0:T(8,128)(2,1)S(1)}, u32[]{:S(2)}, u32[]{:S(2)}) async-start(bf16[32,8,896]{2,1,0:T(8,128)(2,1)} %project_body.1), calls=%async_computation | async-start | bytes 917504 | tf_op jit(solution)/shard_map/all_to_all | solution.py:185
  16.5 0.0 copy-done.2
  16.5 2.9 %collective-permute-start = (bf16[2048,128]{1,0:T(8,128)(2,1)S(1)}, bf16[2048,128]{1,0:T(8,128)(2,1)}, u32[]{:S(2)}, u32[]{:S(2)}) collective-permute-start(bf16[2048,128]{1,0:T(8,128)(2,1)S(1)} %bitcast.37), channel_id=1, source_target_pairs={{0,1},{1,0},{2,3},{3,2},{4,5},{5,4},{6,7},{7,6},{8,9},{9,8},{10,11... | collective-permute-start | bytes 1572872 | tf_op jit(solution)/shard_map/ppermute | solution.py:203
  19.6 0.0 copy-done.13
  19.6 0.1 dynamic-slice.1
  19.7 0.0 copy-done.7
  19.7 0.0 copy-done.12
  19.7 0.1 copy.25
  19.8 0.0 copy-done.11
  19.8 0.0 copy-start.8
  19.8 0.0 copy-done.9
  19.8 0.0 copy-done.10
  19.9 0.7 copy-done.8
  20.5 0.0 copy-start.3
  20.5 2.0 %all-gather = bf16[128,384]{1,0:T(8,128)(2,1)S(1)} all-gather(bf16[64,384]{1,0:T(8,128)(2,1)S(1)} %pad_maximum_fusion), channel_id=2, replica_groups=mesh['z'=8,'x'=4,'y'=8,'c'=2] {'c'}, dimensions={0}, use_global_device_ids=true | all-gather | bytes 147456 | tf_op jit(solution)/shard_map/all_gather | solution.py:280
  22.6 0.0 copy-done.5
  22.6 0.1 dynamic_slice.22
  22.6 0.1 fusion.36
  22.7 0.1 dynamic-slice_bitcast_fusion
  22.8 0.3 fusion.3
  23.1 0.3 fusion.sel_ref
  23.4 0.0 copy-start.6
  23.4 0.2 slice_reduce_fusion.1
  23.6 0.1 maximum_bitcast_fusion
  23.7 0.1 fusion.34
  23.8 0.1 pad_maximum_fusion.1
  23.8 0.3 copy-done.6
  24.2 0.0 collective-permute-done.pg_ref
  24.2 6.8 %all-to-all-done.arr_ref = bf16[32,8,896]{2,1,0:T(8,128)(2,1)S(1)} async-done(((bf16[32,8,896]{2,1,0:T(8,128)(2,1)}), bf16[32,8,896]{2,1,0:T(8,128)(2,1)S(1)}, u32[]{:S(2)}, u32[]{:S(2)}) %all-to-all-start) | async-done | bytes 458784 | tf_op jit(solution)/shard_map/all_to_all | solution.py:185
  31.0 0.1 broadcast_in_dim.81.gain_ref
  31.0 0.1 broadcast_in_dim.80.weight_ref
  31.1 0.0 copy-done.3
  31.1 4.9 %collective-permute-start.1 = (bf16[2048,128]{1,0:T(8,128)(2,1)S(1)}, bf16[2048,128]{1,0:T(8,128)(2,1)}, u32[]{:S(2)}, u32[]{:S(2)}) collective-permute-start(bf16[2048,128]{1,0:T(8,128)(2,1)S(1)} %bitcast.39), channel_id=1, source_target_pairs={{0,1},{1,0},{2,3},{3,2},{4,5},{5,4},{6,7},{7,6},{8,9},{9,8},{10,11... | collective-permute-start | bytes 1572872 | tf_op jit(solution)/shard_map/ppermute | solution.py:203
  36.0 1.9 %collective-permute-start.2 = (bf16[128,2048]{1,0:T(8,128)(2,1)}, bf16[128,2048]{1,0:T(8,128)(2,1)}, u32[]{:S(2)}, u32[]{:S(2)}) collective-permute-start(bf16[128,2048]{1,0:T(8,128)(2,1)} %bitcast.14.ed_ref), channel_id=1, source_target_pairs={{0,1},{1,0},{2,3},{3,2},{4,5},{5,4},{6,7},{7,6},{8,9},{9,8},{10,11... | collective-permute-start | bytes 1572872 | tf_op jit(solution)/shard_map/ppermute | solution.py:203
  38.0 0.0 copy-done.1
  38.0 1.4 %retain_body.1 = (bf16[32,8,256]{2,1,0:T(8,128)(2,1)}, f32[8,128]{1,0:T(8,128)S(1)}, f32[8,256]{1,0:T(8,128)S(1)}) custom-call(bf16[32,8,896]{2,1,0:T(8,128)(2,1)S(1)} %all-to-all-done.arr_ref, f32[8,128,256]{2,1,0:T(8,128)S(1)} %bitcast.34, f32[8,128]{1,0:T(8,128)S(1)} %get-tuple-element.24.cos_ref, f32[8,128]{1,0:T(8,128)S(1)} %get-tuple-element.25.sin_ref, ...), custom_call_target="tpu_custom_call" | custom-call | tf_op jit(solution)/shard_map/retain_body/pallas_call | solution.py:174
  39.3 4.2 %all-to-all-start.1 = ((bf16[32,8,256]{2,1,0:T(8,128)(2,1)}), bf16[32,8,256]{2,1,0:T(8,128)(2,1)S(1)}, u32[]{:S(2)}, u32[]{:S(2)}) async-start(bf16[32,8,256]{2,1,0:T(8,128)(2,1)} %get-tuple-element.27), calls=%async_computation.1 | async-start | bytes 262144 | tf_op jit(solution)/shard_map/all_to_all | solution.py:185
  43.5 1.2 multiply_add_fusion
  44.7 8.2 %all-to-all-done.1 = bf16[32,8,256]{2,1,0:T(8,128)(2,1)S(1)} async-done(((bf16[32,8,256]{2,1,0:T(8,128)(2,1)}), bf16[32,8,256]{2,1,0:T(8,128)(2,1)S(1)}, u32[]{:S(2)}, u32[]{:S(2)}) %all-to-all-start.1) | async-done | bytes 131104 | tf_op jit(solution)/shard_map/all_to_all | solution.py:185
  52.9 0.0 collective-permute-done.1.pu_ref
  52.9 0.0 collective-permute-done.2.pd_ref
  52.9 0.0 copy-done
  52.9 0.2 fusion.1
  53.1 3.6 %all-gather.1 = bf16[128,256]{1,0:T(8,128)(2,1)S(1)} all-gather(bf16[64,256]{1,0:T(8,128)(2,1)S(1)} %fusion.1), channel_id=3, replica_groups=mesh['z'=8,'x'=4,'y'=8,'c'=2] {'c'}, dimensions={0}, use_global_device_ids=true | all-gather | bytes 98304 | tf_op jit(solution)/shard_map/all_gather | solution.py:338
  56.7 14.6 %all_to_all.30 = bf16[8,64,128]{2,1,0:T(8,128)(2,1)S(1)} all-to-all(bf16[8,64,128]{2,1,0:T(8,128)(2,1)S(1)} %broadcast_in_dim.85), channel_id=1, replica_groups=mesh['z'=8,'x'=4,'y'=8,'c'=2] {'y'}, dimensions={0} | all-to-all | bytes 262144 | tf_op jit(solution)/shard_map/all_to_all | solution.py:185
  71.3 0.0 copy-start.4
  71.3 0.3 dispatch_body.1
  71.7 13.7 %all_to_all.31.arr_ref = bf16[32,40,128]{2,1,0:T(8,128)(2,1)S(1)} all-to-all(bf16[32,40,128]{2,1,0:T(8,128)(2,1)S(1)} %dispatch_body.1), channel_id=1, replica_groups=mesh['z'=8,'x'=4,'y'=8,'c'=2] {'z','x'}, dimensions={0} | all-to-all | bytes 655360 | tf_op jit(solution)/shard_map/all_to_all | solution.py:185
  85.4 0.0 copy-done.4
  85.4 2.9 %expert_body.1 = bf16[32,24,128]{2,1,0:T(8,128)(2,1)S(1)} custom-call(bf16[32,40,128]{2,1,0:T(8,128)(2,1)S(1)} %all_to_all.31.arr_ref, f32[1,2048]{1,0:T(1,128)S(1)} %bitcast.41, bf16[2048,128]{1,0:T(8,128)(2,1)S(1)} %bitcast.38, bf16[2048,128]{1,0:T(8,128)(2,1)S(1)} %bitcast.40, bf16[2048,128]{1,0:T(8,128)(2,1)} %collective-permute-done.pg_ref, ...), custom_call_target="tpu_custom_call" | custom-call | tf_op jit(solution)/shard_map/expert_body/pallas_call | solution.py:174
  88.3 15.4 %all_to_all.32.arr_ref = bf16[32,24,128]{2,1,0:T(8,128)(2,1)S(1)} all-to-all(bf16[32,24,128]{2,1,0:T(8,128)(2,1)S(1)} %expert_body.1), channel_id=1, replica_groups=mesh['z'=8,'x'=4,'y'=8,'c'=2] {'z','x'}, dimensions={0} | all-to-all | bytes 393216 | tf_op jit(solution)/shard_map/all_to_all | solution.py:185
  103.6 0.2 collect_body.1
  103.9 11.1 %all_to_all.33 = bf16[8,64,128]{2,1,0:T(8,128)(2,1)S(1)} all-to-all(bf16[8,64,128]{2,1,0:T(8,128)(2,1)S(1)} %broadcast_in_dim.87), channel_id=1, replica_groups=mesh['z'=8,'x'=4,'y'=8,'c'=2] {'y'}, dimensions={0} | all-to-all | bytes 262144 | tf_op jit(solution)/shard_map/all_to_all | solution.py:185
  115.0 6.2 %all-gather.2 = bf16[128,128]{1,0:T(8,128)(2,1)S(1)} all-gather(bf16[64,128]{1,0:T(8,128)(2,1)S(1)} %add_convert_fusion), channel_id=4, replica_groups=mesh['z'=8,'x'=4,'y'=8,'c'=2] {'c'}, dimensions={0}, use_global_device_ids=true | all-gather | bytes 49152 | tf_op jit(solution)/shard_map/all_gather | solution.py:371
  121.2 0.6 copy.29
  (25 shorter events, 0.2 us)
Async XLA Ops:
  0.6 52.3 %copy-start = (bf16[256,64]{0,1:T(8,128)(2,1)S(1)}, bf16[256,64]{0,1:T(8,128)(2,1)}, u32[]{:S(2)}) copy-start(bf16[256,64]{0,1:T(8,128)(2,1)} %param.25) | copy-start | bytes 98308
  0.7 15.9 %copy-start.2 = (bf16[1,2048,128]{2,1,0:T(8,128)(2,1)S(1)}, bf16[1,2048,128]{2,1,0:T(8,128)(2,1)}, u32[]{:S(2)}) copy-start(bf16[1,2048,128]{2,1,0:T(8,128)(2,1)} %param.29) | copy-start | bytes 1572868
  0.7 18.9 %copy-start.13 = (s32[8]{0:T(128)S(1)}, s32[8]{0:T(128)}, u32[]{:S(2)}) copy-start(s32[8]{0:T(128)} %param.27) | copy-start | bytes 100
  0.7 19.0 %copy-start.7 = (s32[256,4]{0,1:T(4,128)S(1)}, s32[256,4]{0,1:T(4,128)}, u32[]{:S(2)}) copy-start(s32[256,4]{0,1:T(4,128)} %param.32) | copy-start | bytes 12292
  0.7 19.0 %copy-start.12 = (bf16[64]{0:T(256)(128)(2,1)S(1)}, bf16[64]{0:T(256)(128)(2,1)}, u32[]{:S(2)}) copy-start(bf16[64]{0:T(256)(128)(2,1)} %param.37) | copy-start | bytes 388
  0.7 19.1 %copy-start.11 = (f32[256,4]{0,1:T(4,128)S(1)}, f32[256,4]{0,1:T(4,128)}, u32[]{:S(2)}) copy-start(f32[256,4]{0,1:T(4,128)} %param.33) | copy-start | bytes 12292
  0.7 19.1 %copy-start.9 = (bf16[64,128]{1,0:T(8,128)(2,1)S(1)}, bf16[64,128]{1,0:T(8,128)(2,1)}, u32[]{:S(2)}) copy-start(bf16[64,128]{1,0:T(8,128)(2,1)} %param.35) | copy-start | bytes 49156
  0.7 19.1 %copy-start.10 = (bf16[64,128]{1,0:T(8,128)(2,1)S(1)}, bf16[64,128]{1,0:T(8,128)(2,1)}, u32[]{:S(2)}) copy-start(bf16[64,128]{1,0:T(8,128)(2,1)} %param.34) | copy-start | bytes 49156
  2.7 35.3 %copy-start.1 = (f32[8,1,128,256]{3,2,1,0:T(8,128)S(1)}, f32[8,1,128,256]{3,2,1,0:T(8,128)}, u32[]{:S(2)}) copy-start(f32[8,1,128,256]{3,2,1,0:T(8,128)} %param.26) | copy-start | bytes 3145732
  2.7 28.3 %all-to-all-start = ((bf16[32,8,896]{2,1,0:T(8,128)(2,1)}), bf16[32,8,896]{2,1,0:T(8,128)(2,1)S(1)}, u32[]{:S(2)}, u32[]{:S(2)}) async-start(bf16[32,8,896]{2,1,0:T(8,128)(2,1)} %project_body.1), calls=%async_computation | async-start | bytes 917504 | tf_op jit(solution)/shard_map/all_to_all | solution.py:185
  16.5 7.6 %collective-permute-start = (bf16[2048,128]{1,0:T(8,128)(2,1)S(1)}, bf16[2048,128]{1,0:T(8,128)(2,1)}, u32[]{:S(2)}, u32[]{:S(2)}) collective-permute-start(bf16[2048,128]{1,0:T(8,128)(2,1)S(1)} %bitcast.37), channel_id=1, source_target_pairs={{0,1},{1,0},{2,3},{3,2},{4,5},{5,4},{6,7},{7,6},{8,9},{9,8},{10,11... | collective-permute-start | bytes 1572872 | tf_op jit(solution)/shard_map/ppermute | solution.py:203
  19.8 0.7 copy-start.8
  20.5 2.0 %copy-start.5 = (f32[2048]{0:T(1024)S(1)}, f32[2048]{0:T(1024)}, u32[]{:S(2)}) copy-start(f32[2048]{0:T(1024)} %param.28) | copy-start | bytes 24580
  20.5 10.6 %copy-start.3 = (bf16[1,2048,128]{2,1,0:T(8,128)(2,1)S(1)}, bf16[1,2048,128]{2,1,0:T(8,128)(2,1)}, u32[]{:S(2)}) copy-start(bf16[1,2048,128]{2,1,0:T(8,128)(2,1)} %param.30) | copy-start | bytes 1572868
  23.4 0.8 copy-start.6
  31.1 21.8 %collective-permute-start.1 = (bf16[2048,128]{1,0:T(8,128)(2,1)S(1)}, bf16[2048,128]{1,0:T(8,128)(2,1)}, u32[]{:S(2)}, u32[]{:S(2)}) collective-permute-start(bf16[2048,128]{1,0:T(8,128)(2,1)S(1)} %bitcast.39), channel_id=1, source_target_pairs={{0,1},{1,0},{2,3},{3,2},{4,5},{5,4},{6,7},{7,6},{8,9},{9,8},{10,11... | collective-permute-start | bytes 1572872 | tf_op jit(solution)/shard_map/ppermute | solution.py:203
  36.0 16.9 %collective-permute-start.2 = (bf16[128,2048]{1,0:T(8,128)(2,1)}, bf16[128,2048]{1,0:T(8,128)(2,1)}, u32[]{:S(2)}, u32[]{:S(2)}) collective-permute-start(bf16[128,2048]{1,0:T(8,128)(2,1)} %bitcast.14.ed_ref), channel_id=1, source_target_pairs={{0,1},{1,0},{2,3},{3,2},{4,5},{5,4},{6,7},{7,6},{8,9},{9,8},{10,11... | collective-permute-start | bytes 1572872 | tf_op jit(solution)/shard_map/ppermute | solution.py:203
  39.3 13.6 %all-to-all-start.1 = ((bf16[32,8,256]{2,1,0:T(8,128)(2,1)}), bf16[32,8,256]{2,1,0:T(8,128)(2,1)S(1)}, u32[]{:S(2)}, u32[]{:S(2)}) async-start(bf16[32,8,256]{2,1,0:T(8,128)(2,1)} %get-tuple-element.27), calls=%async_computation.1 | async-start | bytes 262144 | tf_op jit(solution)/shard_map/all_to_all | solution.py:185
  71.3 14.1 %copy-start.4 = (bf16[1,2048,128]{2,1,0:T(8,128)(2,1)S(1)}, bf16[1,2048,128]{2,1,0:T(8,128)(2,1)}, u32[]{:S(2)}) copy-start(bf16[1,2048,128]{2,1,0:T(8,128)(2,1)} %param.30) | copy-start | bytes 1572868

commit v4 on v3

--- a/solution.py
+++ b/solution.py
@@ -4,6 +4,7 @@
 from jax.experimental import pallas as pl
 from jax.experimental.pallas import tpu as pltpu
 from jax.sharding import Mesh, PartitionSpec as P
+
 
 D = 2048
 KEY_DIM = 128
@@ -98,21 +99,27 @@
     gain_ref,
     eg_ref,
     eu_ref,
+    weight_ref,
     pg_ref,
     pu_ref,
-    weight_ref,
     ed_ref,
     pd_ref,
     out_ref,
     zn_ref,
+    other_gate,
+    other_up,
     own_down,
     other_down,
     sems,
 ):
-    first = pltpu.make_async_copy(ed_ref, own_down, sems.at[0])
-    second = pltpu.make_async_copy(pd_ref, other_down, sems.at[1])
-    first.start()
-    second.start()
+    loads = [
+        pltpu.make_async_copy(pg_ref, other_gate, sems.at[0]),
+        pltpu.make_async_copy(pu_ref, other_up, sems.at[1]),
+        pltpu.make_async_copy(ed_ref, own_down, sems.at[2]),
+        pltpu.make_async_copy(pd_ref, other_down, sems.at[3]),
+    ]
+    for load in loads:
+        load.start()
     tail = jnp.sum(arr_ref[:, 16:40, :].astype(F32), axis=0)
     stats = tail[16:24]
     scale = lax.rsqrt((stats[:, 1:2] + stats[:, 3:4]) / D + EPS)
@@ -144,10 +151,12 @@
         return ((up + 1.0) * gate * jax.nn.sigmoid(ALPHA * gate)).astype(BF16)
 
     own = hidden_of(eg_ref, eu_ref)
-    other = hidden_of(pg_ref, pu_ref)
+    loads[0].wait()
+    loads[1].wait()
+    other = hidden_of(other_gate, other_up)
     weight = weight_ref[...]
-    first.wait()
-    second.wait()
+    loads[2].wait()
+    loads[3].wait()
     for p in range(16):
         at = slice(128 * p, 128 * p + 128)
         o = (mm(own, own_down[:, at]) + mm(other, other_down[:, at])) * weight
@@ -177,7 +186,6 @@
         in_specs=[inside] * len(args) + [outside] * len(far),
         out_specs=[inside] * len(out_shapes),
         scratch_shapes=list(scratch),
-        name=body.__name__,
     )(*args, *far)
 
 
@@ -324,12 +332,12 @@
         sine,
         decay_row,
     )
-    heads = exchange(gated, EP).reshape(256, VAL_DIM)
+    heads = exchange(gated, EP)
+    heads = heads.reshape(256, VAL_DIM)
 
     new_state = decay * prior_state + key_rot[:, None, :, None] * values[:, None, None, :]
-    other_up, other_down, _ = lax.optimization_barrier((expert_up[0], expert_down[0], cosine))
-    other_up = partner(other_up)
-    other_down = partner(other_down)
+    other_up = partner(expert_up[0])
+    other_down = partner(expert_down[0])
     heads, new_state, other_up, other_down = lax.optimization_barrier(
         (heads, new_state, other_up, other_down)
     )
@@ -354,15 +362,15 @@
         ffn_gain[None, :],
         expert_gate[0],
         expert_up[0],
-        other_gate,
-        other_up,
         slot_weight,
-        far=(expert_down[0], other_down),
+        far=(other_gate, other_up, expert_down[0], other_down),
         scratch=(
             pltpu.VMEM((32, D), BF16),
+            pltpu.VMEM((D, 128), BF16),
+            pltpu.VMEM((D, 128), BF16),
             pltpu.VMEM((128, D), BF16),
             pltpu.VMEM((128, D), BF16),
-            pltpu.SemaphoreType.DMA((2,)),
+            pltpu.SemaphoreType.DMA((4,)),
         ),
     )
     returned = exchange(made, EP)
@@ -397,6 +405,7 @@
         P(tp, EP),
         P(EP),
     )
+
     return jax.shard_map(
         per_device,
         mesh=fine,

time: 123 us -> 120 us (0.976)
  waiting for transfers between devices: 15 us -> 9.03 us
  starting transfers between devices: 27.7 us -> 30.1 us
  local copies, waits for them, and re-layouts: 2.18 us -> 4.31 us
    all_to_all x2, waiting for transfers between devices: 15 us -> 9.02 us  [exchange(): return lax.all_to_all(pieces, axes, 0, 0, tiled=True)]
    all_to_all x2, starting transfers between devices: 18 us -> 22.9 us  [exchange(): return lax.all_to_all(pieces, axes, 0, 0, tiled=True)]
    ppermute x3, starting transfers between devices: 9.71 us -> 7.19 us  [partner(): return lax.ppermute(value, 'c', [(0, 1), (1, 0)])]
    unnamed x28, local copies, waits for them, and re-layouts: 1.03 us -> 3.16 us
where the time goes in v4:
time: 120 us; the launch traced here: 119 us
  blocking collectives  65.9 us (55%)
  starting transfers between devices  30.1 us (25%)
  waiting for transfers between devices  9.03 us (8%)
  Pallas kernels  6.02 us (5%)
  local copies, waits for them, and re-layouts  4.31 us (4%)
  other arithmetic  1.89 us (2%)
    all_to_all x4, blocking collectives, exchange(): return lax.all_to_all(pieces, axes, 0, 0, tiled=True)  54.7 us
    all_to_all x2, starting transfers between devices, exchange(): return lax.all_to_all(pieces, axes, 0, 0, tiled=True)  22.9 us
    all_to_all x2, waiting for transfers between devices, exchange(): return lax.all_to_all(pieces, axes, 0, 0, tiled=True)  9.02 us
    ppermute x3, starting transfers between devices, partner(): return lax.ppermute(value, 'c', [(0, 1), (1, 0)])  7.19 us
    all_gather x1, blocking collectives, per_device(): layer_out = lax.all_gather(out_half, 'c')  6.16 us
    pallas_call x5, Pallas kernels, call(): pl.pallas_call(body, out_shape=[pltpu.VMEM(shape, kind) for shape, kind i...  6.02 us
    all_gather x1, blocking collectives, per_device(): pair = own_half(lax.all_gather(attn, 'c'), core, 2).astype(F32)  3.17 us
    unnamed x28, local copies, waits for them, and re-layouts  3.16 us
  transfers between devices with their start and end apart: 5, of which 2 were waited for; matrix products, arithmetic and copies ran while one was open for 2% of the time, Pallas kernels for 1%

profile of v4, /device:TPU:1, one launch (start us, length us, event | category | flops | bytes accessed | tf_op | source)
XLA Modules:
  0.0 119.0 jit_solution(601572750241309440)
XLA Ops:
  0.6 0.0 copy-start
  0.6 0.0 copy-start.2
  0.7 0.0 copy-start.3
  0.7 0.0 copy-start.7
  0.7 0.0 copy-start.11
  0.7 2.0 %shard_map.194 = bf16[32,8,896]{2,1,0:T(8,128)(2,1)} custom-call(bf16[64,256]{1,0:T(8,128)(2,1)} %bitcast.47, f32[1,64]{1,0:T(1,128)} %bitcast.53, bf16[64,128]{1,0:T(8,128)(2,1)} %q_ref.1, bf16[64,128]{1,0:T(8,128)(2,1)} %k_ref.1, bf16[64,256]{1,0:T(8,128)(2,1)} %v_ref.1, bf16[64,256]{1,0:T(8,128)(2,1)} %g_ref.1), custom_call_target="tpu_custom_call" | custom-call | tf_op jit(solution)/shard_map/pallas_call | solution.py:183
  2.7 0.0 copy-start.1
  2.7 13.8 %all-to-all-start = ((bf16[32,8,896]{2,1,0:T(8,128)(2,1)}), bf16[32,8,896]{2,1,0:T(8,128)(2,1)S(1)}, u32[]{:S(2)}, u32[]{:S(2)}) async-start(bf16[32,8,896]{2,1,0:T(8,128)(2,1)} %shard_map.194), calls=%async_computation | async-start | bytes 917504 | tf_op jit(solution)/shard_map/all_to_all | solution.py:193
  16.5 0.0 copy-done.2
  16.6 2.9 %collective-permute-start = (bf16[2048,128]{1,0:T(8,128)(2,1)S(1)}, bf16[2048,128]{1,0:T(8,128)(2,1)S(1)}, u32[]{:S(2)}, u32[]{:S(2)}) collective-permute-start(bf16[2048,128]{1,0:T(8,128)(2,1)S(1)} %bitcast.37), channel_id=1, source_target_pairs={{0,1},{1,0},{2,3},{3,2},{4,5},{5,4},{6,7},{7,6},{8,9},{9,8},{10,11... | collective-permute-start | bytes 1572872 | tf_op jit(solution)/shard_map/ppermute | solution.py:211
  19.4 0.0 copy-done.3
  19.4 1.9 %collective-permute-start.1 = (bf16[2048,128]{1,0:T(8,128)(2,1)S(1)}, bf16[2048,128]{1,0:T(8,128)(2,1)}, u32[]{:S(2)}, u32[]{:S(2)}) collective-permute-start(bf16[2048,128]{1,0:T(8,128)(2,1)S(1)} %bitcast.39), channel_id=1, source_target_pairs={{0,1},{1,0},{2,3},{3,2},{4,5},{5,4},{6,7},{7,6},{8,9},{9,8},{10,11... | collective-permute-start | bytes 1572872 | tf_op jit(solution)/shard_map/ppermute | solution.py:211
  21.4 2.4 %collective-permute-start.2 = (bf16[128,2048]{1,0:T(8,128)(2,1)}, bf16[128,2048]{1,0:T(8,128)(2,1)}, u32[]{:S(2)}, u32[]{:S(2)}) collective-permute-start(bf16[128,2048]{1,0:T(8,128)(2,1)} %bitcast.42), channel_id=1, source_target_pairs={{0,1},{1,0},{2,3},{3,2},{4,5},{5,4},{6,7},{7,6},{8,9},{9,8},{10,11... | collective-permute-start | bytes 1572872 | tf_op jit(solution)/shard_map/ppermute | solution.py:211
  23.9 0.1 dynamic-slice.1
  24.0 0.0 copy-done.7
  24.0 0.0 copy-done.11
  24.0 0.1 dynamic-slice_bitcast_fusion
  24.1 0.3 fusion.3
  24.4 0.0 copy-start.10
  24.4 0.3 fusion.sel_ref
  24.7 0.0 copy-start.8
  24.7 0.0 copy-start.9
  24.7 0.1 fusion.36
  24.8 0.2 slice_reduce_fusion.1
  25.0 0.1 copy-done.10
  25.1 0.3 copy-done.8
  25.4 0.0 copy-done.9
  25.4 0.1 maximum_bitcast_fusion
  25.5 0.0 copy-start.13
  25.6 0.6 copy-done.13
  26.2 0.7 copy-done.12
  26.9 0.1 copy.25
  27.0 0.6 copy-done.4
  27.6 0.1 dynamic_slice.22
  27.6 0.1 fusion.34
  27.8 0.0 copy-start.6
  27.8 1.9 %all-gather = bf16[128,384]{1,0:T(8,128)(2,1)S(1)} all-gather(bf16[64,384]{1,0:T(8,128)(2,1)S(1)} %pad_maximum_fusion), channel_id=2, replica_groups=mesh['z'=8,'x'=4,'y'=8,'c'=2] {'c'}, dimensions={0}, use_global_device_ids=true | all-gather | bytes 147456 | tf_op jit(solution)/shard_map/all_gather | solution.py:288
  29.6 0.1 pad_maximum_fusion.1
  29.7 0.0 copy-done.6
  29.7 0.0 collective-permute-done.pg_ref
  29.7 0.0 copy-start.5
  29.7 0.8 copy-done.5
  30.5 0.5 all-to-all-done.arr_ref
  31.0 0.1 broadcast_in_dim.81.gain_ref
  31.1 0.1 broadcast_in_dim.80.weight_ref
  31.1 0.0 copy-done.1
  31.1 1.4 %shard_map.195 = (bf16[32,8,256]{2,1,0:T(8,128)(2,1)}, f32[8,128]{1,0:T(8,128)S(1)}, f32[8,256]{1,0:T(8,128)S(1)}) custom-call(bf16[32,8,896]{2,1,0:T(8,128)(2,1)S(1)} %all-to-all-done.arr_ref, f32[8,128,256]{2,1,0:T(8,128)S(1)} %bitcast.34, f32[8,128]{1,0:T(8,128)S(1)} %get-tuple-element.22.cos_ref, f32[8,128]{1,0:T(8,128)S(1)} %get-tuple-element.23.sin_ref, ...), custom_call_target="tpu_custom_call" | custom-call | tf_op jit(solution)/shard_map/pallas_call | solution.py:183
  32.5 9.0 %all-to-all-start.1 = ((bf16[32,8,256]{2,1,0:T(8,128)(2,1)}), bf16[32,8,256]{2,1,0:T(8,128)(2,1)S(1)}, u32[]{:S(2)}, u32[]{:S(2)}) async-start(bf16[32,8,256]{2,1,0:T(8,128)(2,1)} %get-tuple-element.25), calls=%async_computation.1 | async-start | bytes 262144 | tf_op jit(solution)/shard_map/all_to_all | solution.py:193
  41.5 1.2 multiply_add_fusion
  42.7 0.0 collective-permute-done.1.pu_ref
  42.7 0.0 collective-permute-done.2.pd_ref
  42.7 8.6 %all-to-all-done.1 = bf16[32,8,256]{2,1,0:T(8,128)(2,1)S(1)} async-done(((bf16[32,8,256]{2,1,0:T(8,128)(2,1)}), bf16[32,8,256]{2,1,0:T(8,128)(2,1)S(1)}, u32[]{:S(2)}, u32[]{:S(2)}) %all-to-all-start.1) | async-done | bytes 131104 | tf_op jit(solution)/shard_map/all_to_all | solution.py:193
  51.3 0.0 copy-done
  51.3 0.2 fusion.1
  51.4 3.2 %all-gather.1 = bf16[128,256]{1,0:T(8,128)(2,1)S(1)} all-gather(bf16[64,256]{1,0:T(8,128)(2,1)S(1)} %fusion.1), channel_id=3, replica_groups=mesh['z'=8,'x'=4,'y'=8,'c'=2] {'c'}, dimensions={0}, use_global_device_ids=true | all-gather | bytes 98304 | tf_op jit(solution)/shard_map/all_gather | solution.py:346
  54.7 14.6 %all_to_all.30 = bf16[8,64,128]{2,1,0:T(8,128)(2,1)S(1)} all-to-all(bf16[8,64,128]{2,1,0:T(8,128)(2,1)S(1)} %broadcast_in_dim.85), channel_id=1, replica_groups=mesh['z'=8,'x'=4,'y'=8,'c'=2] {'y'}, dimensions={0} | all-to-all | bytes 262144 | tf_op jit(solution)/shard_map/all_to_all | solution.py:193
  69.3 0.3 shard_map.196
  69.6 13.8 %all_to_all.31.arr_ref = bf16[32,40,128]{2,1,0:T(8,128)(2,1)S(1)} all-to-all(bf16[32,40,128]{2,1,0:T(8,128)(2,1)S(1)} %shard_map.196), channel_id=1, replica_groups=mesh['z'=8,'x'=4,'y'=8,'c'=2] {'z','x'}, dimensions={0} | all-to-all | bytes 655360 | tf_op jit(solution)/shard_map/all_to_all | solution.py:193
  83.4 2.1 %shard_map.197 = bf16[32,24,128]{2,1,0:T(8,128)(2,1)S(1)} custom-call(bf16[32,40,128]{2,1,0:T(8,128)(2,1)S(1)} %all_to_all.31.arr_ref, f32[1,2048]{1,0:T(1,128)S(1)} %bitcast.41, bf16[2048,128]{1,0:T(8,128)(2,1)S(1)} %bitcast.38, bf16[2048,128]{1,0:T(8,128)(2,1)S(1)} %bitcast.40, f32[32,128]{1,0:T(8,128)S(1)} %broadcast_in_dim.80.weight_ref, ...), custom_call_target="tpu_custom_call" | custom-call | tf_op jit(solution)/shard_map/pallas_call | solution.py:183
  85.5 15.4 %all_to_all.32.arr_ref = bf16[32,24,128]{2,1,0:T(8,128)(2,1)S(1)} all-to-all(bf16[32,24,128]{2,1,0:T(8,128)(2,1)S(1)} %shard_map.197), channel_id=1, replica_groups=mesh['z'=8,'x'=4,'y'=8,'c'=2] {'z','x'}, dimensions={0} | all-to-all | bytes 393216 | tf_op jit(solution)/shard_map/all_to_all | solution.py:193
  100.8 0.2 shard_map.198
  101.1 11.1 %all_to_all.33 = bf16[8,64,128]{2,1,0:T(8,128)(2,1)S(1)} all-to-all(bf16[8,64,128]{2,1,0:T(8,128)(2,1)S(1)} %broadcast_in_dim.87), channel_id=1, replica_groups=mesh['z'=8,'x'=4,'y'=8,'c'=2] {'y'}, dimensions={0} | all-to-all | bytes 262144 | tf_op jit(solution)/shard_map/all_to_all | solution.py:193
  112.2 6.2 %all-gather.2 = bf16[128,128]{1,0:T(8,128)(2,1)S(1)} all-gather(bf16[64,128]{1,0:T(8,128)(2,1)S(1)} %add_convert_fusion), channel_id=4, replica_groups=mesh['z'=8,'x'=4,'y'=8,'c'=2] {'c'}, dimensions={0}, use_global_device_ids=true | all-gather | bytes 49152 | tf_op jit(solution)/shard_map/all_gather | solution.py:379
  118.3 0.6 copy.29
  (25 shorter events, 0.2 us)
Async XLA Ops:
  0.6 50.7 %copy-start = (bf16[256,64]{0,1:T(8,128)(2,1)S(1)}, bf16[256,64]{0,1:T(8,128)(2,1)}, u32[]{:S(2)}) copy-start(bf16[256,64]{0,1:T(8,128)(2,1)} %param.25) | copy-start | bytes 98308
  0.6 15.9 %copy-start.2 = (bf16[1,2048,128]{2,1,0:T(8,128)(2,1)S(1)}, bf16[1,2048,128]{2,1,0:T(8,128)(2,1)}, u32[]{:S(2)}) copy-start(bf16[1,2048,128]{2,1,0:T(8,128)(2,1)} %param.29) | copy-start | bytes 1572868
  0.7 18.8 %copy-start.3 = (bf16[1,2048,128]{2,1,0:T(8,128)(2,1)S(1)}, bf16[1,2048,128]{2,1,0:T(8,128)(2,1)}, u32[]{:S(2)}) copy-start(bf16[1,2048,128]{2,1,0:T(8,128)(2,1)} %param.30) | copy-start | bytes 1572868
  0.7 23.3 %copy-start.7 = (s32[256,4]{0,1:T(4,128)S(1)}, s32[256,4]{0,1:T(4,128)}, u32[]{:S(2)}) copy-start(s32[256,4]{0,1:T(4,128)} %param.32) | copy-start | bytes 12292
  0.7 23.3 %copy-start.11 = (f32[256,4]{0,1:T(4,128)S(1)}, f32[256,4]{0,1:T(4,128)}, u32[]{:S(2)}) copy-start(f32[256,4]{0,1:T(4,128)} %param.33) | copy-start | bytes 12292
  2.7 28.4 %copy-start.1 = (f32[8,1,128,256]{3,2,1,0:T(8,128)S(1)}, f32[8,1,128,256]{3,2,1,0:T(8,128)}, u32[]{:S(2)}) copy-start(f32[8,1,128,256]{3,2,1,0:T(8,128)} %param.26) | copy-start | bytes 3145732
  2.7 28.3 %all-to-all-start = ((bf16[32,8,896]{2,1,0:T(8,128)(2,1)}), bf16[32,8,896]{2,1,0:T(8,128)(2,1)S(1)}, u32[]{:S(2)}, u32[]{:S(2)}) async-start(bf16[32,8,896]{2,1,0:T(8,128)(2,1)} %shard_map.194), calls=%async_computation | async-start | bytes 917504 | tf_op jit(solution)/shard_map/all_to_all | solution.py:193
  16.6 13.2 %collective-permute-start = (bf16[2048,128]{1,0:T(8,128)(2,1)S(1)}, bf16[2048,128]{1,0:T(8,128)(2,1)S(1)}, u32[]{:S(2)}, u32[]{:S(2)}) collective-permute-start(bf16[2048,128]{1,0:T(8,128)(2,1)S(1)} %bitcast.37), channel_id=1, source_target_pairs={{0,1},{1,0},{2,3},{3,2},{4,5},{5,4},{6,7},{7,6},{8,9},{9,8},{10,11... | collective-permute-start | bytes 1572872 | tf_op jit(solution)/shard_map/ppermute | solution.py:211
  19.4 23.3 %collective-permute-start.1 = (bf16[2048,128]{1,0:T(8,128)(2,1)S(1)}, bf16[2048,128]{1,0:T(8,128)(2,1)}, u32[]{:S(2)}, u32[]{:S(2)}) collective-permute-start(bf16[2048,128]{1,0:T(8,128)(2,1)S(1)} %bitcast.39), channel_id=1, source_target_pairs={{0,1},{1,0},{2,3},{3,2},{4,5},{5,4},{6,7},{7,6},{8,9},{9,8},{10,11... | collective-permute-start | bytes 1572872 | tf_op jit(solution)/shard_map/ppermute | solution.py:211
  21.4 21.4 %collective-permute-start.2 = (bf16[128,2048]{1,0:T(8,128)(2,1)}, bf16[128,2048]{1,0:T(8,128)(2,1)}, u32[]{:S(2)}, u32[]{:S(2)}) collective-permute-start(bf16[128,2048]{1,0:T(8,128)(2,1)} %bitcast.42), channel_id=1, source_target_pairs={{0,1},{1,0},{2,3},{3,2},{4,5},{5,4},{6,7},{7,6},{8,9},{9,8},{10,11... | collective-permute-start | bytes 1572872 | tf_op jit(solution)/shard_map/ppermute | solution.py:211
  24.4 0.7 copy-start.10
  24.7 0.7 copy-start.8
  24.7 0.7 copy-start.9
  25.5 0.7 copy-start.13
  26.2 0.7 copy-start.12
  26.9 0.7 copy-start.4
  27.8 2.0 %copy-start.6 = (bf16[256,64]{0,1:T(8,128)(2,1)S(1)}, bf16[256,64]{0,1:T(8,128)(2,1)}, u32[]{:S(2)}) copy-start(bf16[256,64]{0,1:T(8,128)(2,1)} %param.19) | copy-start | bytes 98308
  29.7 0.8 copy-start.5
  32.5 18.8 %all-to-all-start.1 = ((bf16[32,8,256]{2,1,0:T(8,128)(2,1)}), bf16[32,8,256]{2,1,0:T(8,128)(2,1)S(1)}, u32[]{:S(2)}, u32[]{:S(2)}) async-start(bf16[32,8,256]{2,1,0:T(8,128)(2,1)} %get-tuple-element.25), calls=%async_computation.1 | async-start | bytes 262144 | tf_op jit(solution)/shard_map/all_to_all | solution.py:193

commit v5 on v4

--- a/solution.py
+++ b/solution.py
@@ -97,26 +97,22 @@
 def expert_body(
     arr_ref,
     gain_ref,
-    eg_ref,
-    eu_ref,
+    own_ref,
     weight_ref,
-    pg_ref,
-    pu_ref,
+    other_ref,
     ed_ref,
     pd_ref,
     out_ref,
     zn_ref,
-    other_gate,
-    other_up,
+    other_in,
     own_down,
     other_down,
     sems,
 ):
     loads = [
-        pltpu.make_async_copy(pg_ref, other_gate, sems.at[0]),
-        pltpu.make_async_copy(pu_ref, other_up, sems.at[1]),
-        pltpu.make_async_copy(ed_ref, own_down, sems.at[2]),
-        pltpu.make_async_copy(pd_ref, other_down, sems.at[3]),
+        pltpu.make_async_copy(other_ref, other_in, sems.at[0]),
+        pltpu.make_async_copy(ed_ref, own_down, sems.at[1]),
+        pltpu.make_async_copy(pd_ref, other_down, sems.at[2]),
     ]
     for load in loads:
         load.start()
@@ -145,18 +141,18 @@
     norm = lax.rsqrt(jnp.sum(squares, axis=1, keepdims=True) / D + EPS)
     zn = zn_ref[...]
 
-    def hidden_of(gate_w, up_w):
-        gate = jnp.minimum(mm(zn, gate_w[...]) * norm, LIMIT)
-        up = jnp.clip(mm(zn, up_w[...]) * norm, -LIMIT, LIMIT)
+    def hidden_of(weights):
+        both = mm(zn, weights[...]) * norm
+        gate = jnp.minimum(both[:, :128], LIMIT)
+        up = jnp.clip(both[:, 128:], -LIMIT, LIMIT)
         return ((up + 1.0) * gate * jax.nn.sigmoid(ALPHA * gate)).astype(BF16)
 
-    own = hidden_of(eg_ref, eu_ref)
+    own = hidden_of(own_ref)
     loads[0].wait()
+    other = hidden_of(other_in)
+    weight = weight_ref[...]
     loads[1].wait()
-    other = hidden_of(other_gate, other_up)
-    weight = weight_ref[...]
     loads[2].wait()
-    loads[3].wait()
     for p in range(16):
         at = slice(128 * p, 128 * p + 128)
         o = (mm(own, own_down[:, at]) + mm(other, other_down[:, at])) * weight
@@ -286,7 +282,8 @@
     mix_block = jnp.pad(mix_vector[:, None], ((0, 0), (0, 127)))
     dense = jnp.concatenate([dense_gate, dense_up, dense_down.T], axis=1)
     dense = lax.all_gather(dense, "c")
-    other_gate = partner(expert_gate[0])
+    own_in = jnp.concatenate([expert_gate[0], expert_up[0]], axis=1)
+    other_in = partner(own_in)
     residual_half = own_half(residual.T, core, 1).astype(F32)
     inverse = 1.0 / 10000.0 ** jnp.linspace(0.0, 1.0, 64, dtype=F32)
     angles = lengths.astype(F32)[:, None] * inverse[None, :]
@@ -303,7 +300,7 @@
         gain_here,
         mix_block,
         dense,
-        other_gate,
+        other_in,
         residual_half,
         cosine,
         sine,
@@ -316,7 +313,7 @@
             gain_here,
             mix_block,
             dense,
-            other_gate,
+            other_in,
             residual_half,
             cosine,
             sine,
@@ -336,11 +333,8 @@
     heads = heads.reshape(256, VAL_DIM)
 
     new_state = decay * prior_state + key_rot[:, None, :, None] * values[:, None, None, :]
-    other_up = partner(expert_up[0])
     other_down = partner(expert_down[0])
-    heads, new_state, other_up, other_down = lax.optimization_barrier(
-        (heads, new_state, other_up, other_down)
-    )
+    heads, new_state, other_down = lax.optimization_barrier((heads, new_state, other_down))
 
     attn = dots(out_weight.T, heads, 1, 1).astype(BF16)
     pair = own_half(lax.all_gather(attn, "c"), core, 2).astype(F32)
@@ -360,17 +354,15 @@
         [((32, 24, 128), BF16)],
         inbox,
         ffn_gain[None, :],
-        expert_gate[0],
-        expert_up[0],
+        own_in,
         slot_weight,
-        far=(other_gate, other_up, expert_down[0], other_down),
+        far=(other_in, expert_down[0], other_down),
         scratch=(
             pltpu.VMEM((32, D), BF16),
-            pltpu.VMEM((D, 128), BF16),
-            pltpu.VMEM((D, 128), BF16),
+            pltpu.VMEM((D, 256), BF16),
             pltpu.VMEM((128, D), BF16),
             pltpu.VMEM((128, D), BF16),
-            pltpu.SemaphoreType.DMA((4,)),
+            pltpu.SemaphoreType.DMA((3,)),
         ),
     )
     returned = exchange(made, EP)

time: 120 us -> 117 us (0.975)
  starting transfers between devices: 30.1 us -> 24.4 us
  waiting for transfers between devices: 9.03 us -> 13.6 us
  local copies, waits for them, and re-layouts: 4.31 us -> 1.24 us
  blocking collectives: 65.9 us -> 67.2 us
    all_to_all x2, waiting for transfers between devices: 9.02 us -> 13.6 us  [exchange(): return lax.all_to_all(pieces, axes, 0, 0, tiled=True)]
    all_to_all x2, starting transfers between devices: 22.9 us -> 19.4 us  [exchange(): return lax.all_to_all(pieces, axes, 0, 0, tiled=True)]
    unnamed x28 -> x26, local copies, waits for them, and re-layouts: 3.16 us -> 0.08 us
    ppermute x3 -> x2, starting transfers between devices: 7.19 us -> 4.92 us  [partner(): return lax.ppermute(value, 'c', [(0, 1), (1, 0)])]
    all_gather x1, blocking collectives: 3.17 us -> 4.56 us  [per_device(): pair = own_half(lax.all_gather(attn, 'c'), core, 2).astype(F32)]
  transfers between devices with their start and end apart: 5 -> 4, of which waited for: 2 -> 2; matrix products, arithmetic and copies ran while one was open for 2% -> 3% of each run, Pallas kernels for 1% -> 1%
where the time goes in v5:
time: 117 us
  blocking collectives  67.2 us (57%)
  starting transfers between devices  24.4 us (21%)
  waiting for transfers between devices  13.6 us (12%)
  Pallas kernels  6.39 us (5%)
  other arithmetic  2.01 us (2%)
  local copies, waits for them, and re-layouts  1.24 us (1%)
    all_to_all x4, blocking collectives, exchange(): return lax.all_to_all(pieces, axes, 0, 0, tiled=True)  54.6 us
    all_to_all x2, starting transfers between devices, exchange(): return lax.all_to_all(pieces, axes, 0, 0, tiled=True)  19.4 us
    all_to_all x2, waiting for transfers between devices, exchange(): return lax.all_to_all(pieces, axes, 0, 0, tiled=True)  13.6 us
    pallas_call x5, Pallas kernels, call(): pl.pallas_call(body, out_shape=[pltpu.VMEM(shape, kind) for shape, kind i...  6.39 us
    all_gather x1, blocking collectives, per_device(): layer_out = lax.all_gather(out_half, 'c')  6.09 us
    ppermute x2, starting transfers between devices, partner(): return lax.ppermute(value, 'c', [(0, 1), (1, 0)])  4.92 us
    all_gather x1, blocking collectives, per_device(): pair = own_half(lax.all_gather(attn, 'c'), core, 2).astype(F32)  4.56 us
  transfers between devices with their start and end apart: 4, of which 2 were waited for; matrix products, arithmetic and copies ran while one was open for 3% of the time, Pallas kernels for 1%

profile of v5, /device:TPU:1, one launch (start us, length us, event | category | flops | bytes accessed | tf_op | source)
XLA Modules:
  0.0 116.6 jit_solution(3477558492763250327)
XLA Ops:
  0.6 0.0 copy-start
  0.6 0.0 copy-start.3
  0.7 0.0 copy-start.4
  0.7 2.0 %shard_map.194 = bf16[32,8,896]{2,1,0:T(8,128)(2,1)} custom-call(bf16[64,256]{1,0:T(8,128)(2,1)} %bitcast.43, f32[1,64]{1,0:T(1,128)} %bitcast.49, bf16[64,128]{1,0:T(8,128)(2,1)} %q_ref.1, bf16[64,128]{1,0:T(8,128)(2,1)} %k_ref.1, bf16[64,256]{1,0:T(8,128)(2,1)} %v_ref.1, bf16[64,256]{1,0:T(8,128)(2,1)} %g_ref.1), custom_call_target="tpu_custom_call" | custom-call | tf_op jit(solution)/shard_map/pallas_call | solution.py:179
  2.7 13.7 %all-to-all-start = ((bf16[32,8,896]{2,1,0:T(8,128)(2,1)}), bf16[32,8,896]{2,1,0:T(8,128)(2,1)S(1)}, u32[]{:S(2)}, u32[]{:S(2)}) async-start(bf16[32,8,896]{2,1,0:T(8,128)(2,1)} %shard_map.194), calls=%async_computation | async-start | bytes 917504 | tf_op jit(solution)/shard_map/all_to_all | solution.py:189
  16.4 2.9 %collective-permute-start.1 = (bf16[128,2048]{1,0:T(8,128)(2,1)}, bf16[128,2048]{1,0:T(8,128)(2,1)}, u32[]{:S(2)}, u32[]{:S(2)}) collective-permute-start(bf16[128,2048]{1,0:T(8,128)(2,1)} %bitcast.14.ed_ref), channel_id=1, source_target_pairs={{0,1},{1,0},{2,3},{3,2},{4,5},{5,4},{6,7},{7,6},{8,9},{9,8},{10,11... | collective-permute-start | bytes 1572872 | tf_op jit(solution)/shard_map/ppermute | solution.py:207
  19.3 0.0 copy-done.3
  19.3 0.0 copy-done.4
  19.3 0.0 copy-start.6
  19.3 0.0 copy-start.10
  19.3 0.0 copy-start.12
  19.3 0.0 copy-start.11
  19.3 0.0 copy-start.2
  19.3 0.0 copy-start.7
  19.4 0.0 copy-start.8
  19.4 0.0 copy-start.9
  19.4 0.1 pad_maximum_fusion.own_ref
  19.5 0.0 copy-start.5
  19.5 0.0 copy-start.1
  19.5 2.1 %collective-permute-start = (bf16[2048,256]{1,0:T(8,128)(2,1)S(1)}, bf16[2048,256]{1,0:T(8,128)(2,1)}, u32[]{:S(2)}, u32[]{:S(2)}) collective-permute-start(bf16[2048,256]{1,0:T(8,128)(2,1)S(1)} %pad_maximum_fusion.own_ref), channel_id=1, source_target_pairs={{0,1},{1,0},{2,3},{3,2},{4,5},{5,4},{6,7},{7,6},{8,9},{9,8},{10,11... | collective-permute-start | bytes 3145736 | tf_op jit(solution)/shard_map/ppermute | solution.py:207
  21.7 0.1 dynamic-slice.1
  21.8 0.0 copy-done.6
  21.8 0.0 copy-done.10
  21.8 0.1 dynamic-slice_bitcast_fusion
  21.9 0.3 fusion.3
  22.2 0.3 fusion.sel_ref
  22.5 0.0 copy-done.12
  22.6 0.0 copy-done.11
  22.6 0.1 copy.25
  22.7 0.0 copy-done.2
  22.7 0.1 dynamic_slice.22
  22.8 0.1 fusion.36
  22.9 0.2 slice_reduce_fusion.1
  23.0 0.1 maximum_bitcast_fusion
  23.1 0.0 copy-done.7
  23.1 0.0 copy-done.8
  23.1 0.0 copy-done.9
  23.2 0.1 fusion.34
  23.3 2.0 %all-gather = bf16[128,384]{1,0:T(8,128)(2,1)S(1)} all-gather(bf16[64,384]{1,0:T(8,128)(2,1)S(1)} %pad_maximum_fusion.1), channel_id=2, replica_groups=mesh['z'=8,'x'=4,'y'=8,'c'=2] {'c'}, dimensions={0}, use_global_device_ids=true | all-gather | bytes 147456 | tf_op jit(solution)/shard_map/all_gather | solution.py:284
  25.3 0.1 pad_maximum_fusion.2
  25.4 0.0 copy-done.5
  25.4 5.5 %all-to-all-done.arr_ref = bf16[32,8,896]{2,1,0:T(8,128)(2,1)S(1)} async-done(((bf16[32,8,896]{2,1,0:T(8,128)(2,1)}), bf16[32,8,896]{2,1,0:T(8,128)(2,1)S(1)}, u32[]{:S(2)}, u32[]{:S(2)}) %all-to-all-start) | async-done | bytes 458784 | tf_op jit(solution)/shard_map/all_to_all | solution.py:189
  30.9 0.0 collective-permute-done.other_ref
  30.9 0.1 broadcast_in_dim.81.gain_ref
  30.9 0.1 broadcast_in_dim.80.weight_ref
  31.0 0.0 copy-done.1
  31.0 1.4 %shard_map.195 = (bf16[32,8,256]{2,1,0:T(8,128)(2,1)}, f32[8,128]{1,0:T(8,128)S(1)}, f32[8,256]{1,0:T(8,128)S(1)}) custom-call(bf16[32,8,896]{2,1,0:T(8,128)(2,1)S(1)} %all-to-all-done.arr_ref, f32[8,128,256]{2,1,0:T(8,128)S(1)} %bitcast.34, f32[8,128]{1,0:T(8,128)S(1)} %get-tuple-element.21.cos_ref, f32[8,128]{1,0:T(8,128)S(1)} %get-tuple-element.22.sin_ref, ...), custom_call_target="tpu_custom_call" | custom-call | tf_op jit(solution)/shard_map/pallas_call | solution.py:179
  32.4 5.7 %all-to-all-start.1 = ((bf16[32,8,256]{2,1,0:T(8,128)(2,1)}), bf16[32,8,256]{2,1,0:T(8,128)(2,1)S(1)}, u32[]{:S(2)}, u32[]{:S(2)}) async-start(bf16[32,8,256]{2,1,0:T(8,128)(2,1)} %get-tuple-element.24), calls=%async_computation.1 | async-start | bytes 262144 | tf_op jit(solution)/shard_map/all_to_all | solution.py:189
  38.1 1.2 %multiply_add_fusion = f32[8,1,128,256]{3,2,1,0:T(8,128)} fusion(f32[8,1,128,256]{3,2,1,0:T(8,128)S(1)} %copy-done.1, f32[8,256]{1,0:T(8,128)S(1)} %get-tuple-element.26, f32[8,128]{1,0:T(8,128)S(1)} %get-tuple-element.25, f32[]{:T(128)S(6)} %sub.44), kind=kLoop, calls=%fused_computation.5 | loop fusion | flops 786432 | bytes 2109444 | tf_op jit(solution)/shard_map/add | solution.py:335
  39.3 0.0 collective-permute-done.1.pd_ref
  39.3 8.2 %all-to-all-done.1 = bf16[32,8,256]{2,1,0:T(8,128)(2,1)S(1)} async-done(((bf16[32,8,256]{2,1,0:T(8,128)(2,1)}), bf16[32,8,256]{2,1,0:T(8,128)(2,1)S(1)}, u32[]{:S(2)}, u32[]{:S(2)}) %all-to-all-start.1) | async-done | bytes 131104 | tf_op jit(solution)/shard_map/all_to_all | solution.py:189
  47.4 0.0 copy-done
  47.4 0.2 fusion.1
  47.6 4.6 %all-gather.1 = bf16[128,256]{1,0:T(8,128)(2,1)S(1)} all-gather(bf16[64,256]{1,0:T(8,128)(2,1)S(1)} %fusion.1), channel_id=3, replica_groups=mesh['z'=8,'x'=4,'y'=8,'c'=2] {'c'}, dimensions={0}, use_global_device_ids=true | all-gather | bytes 98304 | tf_op jit(solution)/shard_map/all_gather | solution.py:340
  52.2 14.6 %all_to_all.30 = bf16[8,64,128]{2,1,0:T(8,128)(2,1)S(1)} all-to-all(bf16[8,64,128]{2,1,0:T(8,128)(2,1)S(1)} %broadcast_in_dim.85), channel_id=1, replica_groups=mesh['z'=8,'x'=4,'y'=8,'c'=2] {'y'}, dimensions={0} | all-to-all | bytes 262144 | tf_op jit(solution)/shard_map/all_to_all | solution.py:189
  66.8 0.3 shard_map.196
  67.1 14.3 %all_to_all.31.arr_ref = bf16[32,40,128]{2,1,0:T(8,128)(2,1)S(1)} all-to-all(bf16[32,40,128]{2,1,0:T(8,128)(2,1)S(1)} %shard_map.196), channel_id=1, replica_groups=mesh['z'=8,'x'=4,'y'=8,'c'=2] {'z','x'}, dimensions={0} | all-to-all | bytes 655360 | tf_op jit(solution)/shard_map/all_to_all | solution.py:189
  81.4 2.4 %shard_map.197 = bf16[32,24,128]{2,1,0:T(8,128)(2,1)S(1)} custom-call(bf16[32,40,128]{2,1,0:T(8,128)(2,1)S(1)} %all_to_all.31.arr_ref, f32[1,2048]{1,0:T(1,128)S(1)} %bitcast.37, bf16[2048,256]{1,0:T(8,128)(2,1)S(1)} %pad_maximum_fusion.own_ref, f32[32,128]{1,0:T(8,128)S(1)} %broadcast_in_dim.80.weight_ref, ...), custom_call_target="tpu_custom_call" | custom-call | tf_op jit(solution)/shard_map/pallas_call | solution.py:179
  83.9 15.0 %all_to_all.32.arr_ref = bf16[32,24,128]{2,1,0:T(8,128)(2,1)S(1)} all-to-all(bf16[32,24,128]{2,1,0:T(8,128)(2,1)S(1)} %shard_map.197), channel_id=1, replica_groups=mesh['z'=8,'x'=4,'y'=8,'c'=2] {'z','x'}, dimensions={0} | all-to-all | bytes 393216 | tf_op jit(solution)/shard_map/all_to_all | solution.py:189
  98.9 0.2 shard_map.198
  99.1 10.8 %all_to_all.33 = bf16[8,64,128]{2,1,0:T(8,128)(2,1)S(1)} all-to-all(bf16[8,64,128]{2,1,0:T(8,128)(2,1)S(1)} %broadcast_in_dim.87), channel_id=1, replica_groups=mesh['z'=8,'x'=4,'y'=8,'c'=2] {'y'}, dimensions={0} | all-to-all | bytes 262144 | tf_op jit(solution)/shard_map/all_to_all | solution.py:189
  109.9 6.1 %all-gather.2 = bf16[128,128]{1,0:T(8,128)(2,1)S(1)} all-gather(bf16[64,128]{1,0:T(8,128)(2,1)S(1)} %add_convert_fusion), channel_id=4, replica_groups=mesh['z'=8,'x'=4,'y'=8,'c'=2] {'c'}, dimensions={0}, use_global_device_ids=true | all-gather | bytes 49152 | tf_op jit(solution)/shard_map/all_gather | solution.py:371
  116.0 0.6 copy.29
  (23 shorter events, 0.2 us)
Async XLA Ops:
  0.6 46.8 %copy-start = (bf16[256,64]{0,1:T(8,128)(2,1)S(1)}, bf16[256,64]{0,1:T(8,128)(2,1)}, u32[]{:S(2)}) copy-start(bf16[256,64]{0,1:T(8,128)(2,1)} %param.25) | copy-start | bytes 98308
  0.6 18.6 %copy-start.3 = (bf16[1,2048,128]{2,1,0:T(8,128)(2,1)S(1)}, bf16[1,2048,128]{2,1,0:T(8,128)(2,1)}, u32[]{:S(2)}) copy-start(bf16[1,2048,128]{2,1,0:T(8,128)(2,1)} %param.30) | copy-start | bytes 1572868
  0.7 18.6 %copy-start.4 = (bf16[1,2048,128]{2,1,0:T(8,128)(2,1)S(1)}, bf16[1,2048,128]{2,1,0:T(8,128)(2,1)}, u32[]{:S(2)}) copy-start(bf16[1,2048,128]{2,1,0:T(8,128)(2,1)} %param.29) | copy-start | bytes 1572868
  2.7 28.2 %all-to-all-start = ((bf16[32,8,896]{2,1,0:T(8,128)(2,1)}), bf16[32,8,896]{2,1,0:T(8,128)(2,1)S(1)}, u32[]{:S(2)}, u32[]{:S(2)}) async-start(bf16[32,8,896]{2,1,0:T(8,128)(2,1)} %shard_map.194), calls=%async_computation | async-start | bytes 917504 | tf_op jit(solution)/shard_map/all_to_all | solution.py:189
  16.4 22.9 %collective-permute-start.1 = (bf16[128,2048]{1,0:T(8,128)(2,1)}, bf16[128,2048]{1,0:T(8,128)(2,1)}, u32[]{:S(2)}, u32[]{:S(2)}) collective-permute-start(bf16[128,2048]{1,0:T(8,128)(2,1)} %bitcast.14.ed_ref), channel_id=1, source_target_pairs={{0,1},{1,0},{2,3},{3,2},{4,5},{5,4},{6,7},{7,6},{8,9},{9,8},{10,11... | collective-permute-start | bytes 1572872 | tf_op jit(solution)/shard_map/ppermute | solution.py:207
  19.3 2.5 %copy-start.6 = (s32[256,4]{0,1:T(4,128)S(1)}, s32[256,4]{0,1:T(4,128)}, u32[]{:S(2)}) copy-start(s32[256,4]{0,1:T(4,128)} %param.32) | copy-start | bytes 12292
  19.3 2.5 %copy-start.10 = (f32[256,4]{0,1:T(4,128)S(1)}, f32[256,4]{0,1:T(4,128)}, u32[]{:S(2)}) copy-start(f32[256,4]{0,1:T(4,128)} %param.33) | copy-start | bytes 12292
  19.3 3.2 %copy-start.12 = (s32[8]{0:T(128)S(1)}, s32[8]{0:T(128)}, u32[]{:S(2)}) copy-start(s32[8]{0:T(128)} %param.27) | copy-start | bytes 100
  19.3 3.2 %copy-start.11 = (bf16[64]{0:T(256)(128)(2,1)S(1)}, bf16[64]{0:T(256)(128)(2,1)}, u32[]{:S(2)}) copy-start(bf16[64]{0:T(256)(128)(2,1)} %param.37) | copy-start | bytes 388
  19.3 3.3 %copy-start.2 = (f32[2048]{0:T(1024)S(1)}, f32[2048]{0:T(1024)}, u32[]{:S(2)}) copy-start(f32[2048]{0:T(1024)} %param.28) | copy-start | bytes 24580
  19.3 3.8 %copy-start.7 = (bf16[128,64]{0,1:T(8,128)(2,1)S(1)}, bf16[128,64]{0,1:T(8,128)(2,1)}, u32[]{:S(2)}) copy-start(bf16[128,64]{0,1:T(8,128)(2,1)} %param.36) | copy-start | bytes 49156
  19.4 3.8 %copy-start.8 = (bf16[64,128]{1,0:T(8,128)(2,1)S(1)}, bf16[64,128]{1,0:T(8,128)(2,1)}, u32[]{:S(2)}) copy-start(bf16[64,128]{1,0:T(8,128)(2,1)} %param.35) | copy-start | bytes 49156
  19.4 3.8 %copy-start.9 = (bf16[64,128]{1,0:T(8,128)(2,1)S(1)}, bf16[64,128]{1,0:T(8,128)(2,1)}, u32[]{:S(2)}) copy-start(bf16[64,128]{1,0:T(8,128)(2,1)} %param.34) | copy-start | bytes 49156
  19.5 5.9 %copy-start.5 = (bf16[256,64]{0,1:T(8,128)(2,1)S(1)}, bf16[256,64]{0,1:T(8,128)(2,1)}, u32[]{:S(2)}) copy-start(bf16[256,64]{0,1:T(8,128)(2,1)} %param.19) | copy-start | bytes 98308
  19.5 11.5 %copy-start.1 = (f32[8,1,128,256]{3,2,1,0:T(8,128)S(1)}, f32[8,1,128,256]{3,2,1,0:T(8,128)}, u32[]{:S(2)}) copy-start(f32[8,1,128,256]{3,2,1,0:T(8,128)} %param.26) | copy-start | bytes 3145732
  19.5 11.3 %collective-permute-start = (bf16[2048,256]{1,0:T(8,128)(2,1)S(1)}, bf16[2048,256]{1,0:T(8,128)(2,1)}, u32[]{:S(2)}, u32[]{:S(2)}) collective-permute-start(bf16[2048,256]{1,0:T(8,128)(2,1)S(1)} %pad_maximum_fusion.own_ref), channel_id=1, source_target_pairs={{0,1},{1,0},{2,3},{3,2},{4,5},{5,4},{6,7},{7,6},{8,9},{9,8},{10,11... | collective-permute-start | bytes 3145736 | tf_op jit(solution)/shard_map/ppermute | solution.py:207
  32.4 15.1 %all-to-all-start.1 = ((bf16[32,8,256]{2,1,0:T(8,128)(2,1)}), bf16[32,8,256]{2,1,0:T(8,128)(2,1)S(1)}, u32[]{:S(2)}, u32[]{:S(2)}) async-start(bf16[32,8,256]{2,1,0:T(8,128)(2,1)} %get-tuple-element.24), calls=%async_computation.1 | async-start | bytes 262144 | tf_op jit(solution)/shard_map/all_to_all | solution.py:189
